TPU v7x, 32 devices: a whole 2x2x4 slice. The times are simulated.
32 devices in a mesh: sp: 8 (over z, y), tp: 4 (over x, core).
Axes of the slice: x: 2, y: 2, z: 4, core: 2. Of those that a mesh axis runs over, the one named last changes fastest.
Arguments:
- mixer_input: bfloat16 [2048, 1024], P('sp', 'tp'), may hold values from -6 to 6
- retention: float32 [64, 2048], P('tp', 'sp'), may hold values from -1 to 0
- decay_real: float32 [64, 64], P('tp'), may hold values from -0.7 to -0.3
- decay_freq: float32 [64, 64], P('tp'), may hold values from 0 to 26
- log_step: float32 [64], P('tp')
- input_real: float32 [64, 64, 16], P('tp')
- input_imag: float32 [64, 64, 16], P('tp')
- readout_real: float32 [64, 16, 64], P('tp'), may hold values from -0.5 to 0.5
- readout_imaginary: float32 [64, 16, 64], P('tp'), may hold values from -0.5 to 0.5
- skip_weight: float32 [64, 16], P('tp'), may hold values from -4 to 4
- norm_gain: float32 [1024], replicated, may hold values from 0.1 to 1.9
- projection: bfloat16 [1024, 2048], P('tp'), may hold values from -0.1875 to 0.1875
- residual: bfloat16 [2048, 2048], P(('sp', 'tp')), may hold values from -6 to 6
- mix_gain: float32 [2048], replicated, may hold values from 0.1 to 1.9
- routes: int32 [2048, 2], P(('sp', 'tp')), may hold values from 0 to 7, all different within a row; in each aligned block of 64 rows (0 to 63, 64 to 127, ...) at most 32 rows name the same one
- route_weight: float32 [2048, 2], P(('sp', 'tp')), may hold values from 0.5 to 2
- expert_gate: bfloat16 [8, 2048, 512], P('sp'), may hold values from -0.125 to 0.125
- expert_up: bfloat16 [8, 2048, 512], P('sp'), may hold values from -0.125 to 0.125
- expert_down: bfloat16 [8, 512, 2048], P('sp'), may hold values from -0.25 to 0.25
- final_gain: float32 [2048], replicated, may hold values from 0.1 to 1.9
Outputs:
- layer_out: bfloat16 [2048, 2048], P(('sp', 'tp'))
Inputs may be any that keep to these rules, and one draw needn't show every extreme that they name: `routes`: in each aligned block of 64 rows no expert is named by more than 32 rows, and in some blocks one is named by exactly 32 rows; each row names 2 different experts.
All inputs are finite; a program needn't handle non-finite values.
Results may differ from a plain program's by a relative error of at most 0.017.
Values may be sent and summed in bfloat16 or wider, within the bound.
A program may use at most 64 MiB of HBM per device.

v0:
```python
import functools

import jax
import jax.numpy as jnp
from jax import lax
from jax.experimental import pallas as pl
from jax.experimental.pallas import tpu as pltpu
from jax.sharding import PartitionSpec as P

PICKS = 2
SPANS = 8
deep_alpha = 2.0**0.25
f32, bf16 = jnp.float32, jnp.bfloat16
highest = lax.Precision.HIGHEST
NT = (((1,), (1,)), ((), ()))
TN = (((0,), (0,)), ((), ()))
PROJ_CHUNKS = 4


def dot(a, b, dims=None, precision=None):
    dims = dims or (((1,), (0,)), ((), ()))
    return lax.dot_general(a, b, dims, precision=precision, preferred_element_type=f32)


def split(value):
    high = value.astype(bf16)
    return high, (value - high.astype(f32)).astype(bf16)


def iota(shape, dim):
    return lax.broadcasted_iota(jnp.int32, shape, dim)


def layer_norm(values, scales):
    centered = values - jnp.mean(values, axis=-1, keepdims=True)
    variance = jnp.mean(centered * centered, axis=-1, keepdims=True)
    return centered * lax.rsqrt(variance + 1e-05) * scales


def cmul(ar, ai, br, bi):
    return ar * br - ai * bi, ar * bi + ai * br


def repeat(count, body):
    if count <= 8:
        for k in range(count):
            body(k)
    else:
        lax.fori_loop(0, count, lambda k, c: (body(k), c)[1], 0)


def kernel(
    n_sp, n_tp, groups, channels, states, cap,
    x_ref, ret_ref, par_ref, skip_ref, gain_ref, in_re_ref, in_im_ref, out_re_ref, out_im_ref,
    res_ref, mix_gain_ref, routes_ref, rw_ref, final_gain_ref, proj_ref, gate_ref, up_ref, down_ref,
    o_ref,
    d_re, d_im, shr, carry_out, carry_in, mix_out, mix_in, proj_all, gate_v, up_v, down_v,
    acc, hid, tok_out, tok_in, ret_out, ret_in,
    w_sem, car_s, car_r, mix_s, mix_r, prj_s, prj_r, fwd_s, fwd_r, tok_s, tok_r, back_s, back_r,
):
    sp, tp = lax.axis_index("sp"), lax.axis_index("tp")
    tokens, chans = x_ref.shape
    gp = groups * states
    span = tokens // SPANS
    rows = tokens // n_tp
    width = o_ref.shape[1]

    barrier = pltpu.get_barrier_semaphore()

    def greet_sp(k):
        pl.semaphore_signal(barrier, inc=1, device_id={"sp": lax.rem(sp + k + 1, n_sp)})

    def greet_tp(k):
        pl.semaphore_signal(barrier, inc=1, device_id={"tp": lax.rem(tp + k + 1, n_tp)})

    repeat(n_sp - 1, greet_sp)
    repeat(n_tp - 1, greet_tp)

    own = pltpu.make_async_copy(proj_ref, proj_all.at[tp], w_sem.at[0])
    own.start()
    loads = [own]
    for i, (src, dst) in enumerate(((gate_ref, gate_v), (up_ref, up_v), (down_ref, down_v))):
        loads.append(pltpu.make_async_copy(src.at[0], dst, w_sem.at[i + 1]))
        loads[-1].start()
    pl.semaphore_wait(barrier, n_sp - 1 + n_tp - 1)

    depth = proj_ref.shape[0] // PROJ_CHUNKS
    near = tp + 1 - 2 * lax.rem(tp, 2)
    far = lax.rem(tp + 2, n_tp)

    def piece(i):
        return pl.ds(i * depth, depth)

    proj_far = [
        pltpu.make_async_remote_copy(
            proj_ref.at[piece(i)], proj_all.at[tp, piece(i)], prj_s.at[i], prj_r.at[i],
            device_id={"tp": far},
        )
        for i in range(PROJ_CHUNKS)
    ]
    proj_near = pltpu.make_async_remote_copy(
        proj_ref, proj_all.at[tp], prj_s.at[PROJ_CHUNKS], prj_r.at[PROJ_CHUNKS],
        device_id={"tp": near},
    )
    proj_fwd = [
        pltpu.make_async_remote_copy(
            proj_all.at[far, piece(i)], proj_all.at[far, piece(i)], fwd_s.at[i], fwd_r.at[i],
            device_id={"tp": near},
        )
        for i in range(PROJ_CHUNKS)
    ]
    for copy in proj_far:
        copy.start()
    proj_near.start()

    row_i, col_i = iota((tokens, tokens), 0), iota((tokens, tokens), 1)
    perm = jnp.where(
        col_i == lax.rem(row_i, SPANS) * span + row_i // SPANS, 1.0, 0.0
    ).astype(bf16)
    x = dot(perm, x_ref[...]).astype(bf16)
    tile_c = jnp.where(
        lax.rem(iota((channels, chans), 1), channels) == iota((channels, chans), 0), 1.0, 0.0
    ).astype(bf16)
    mask_in = iota((gp, chans), 0) // states == iota((gp, chans), 1) // channels

    def drive(ref):
        high, low = split(ref[...])
        wide_high = jnp.where(mask_in, dot(high, tile_c), 0.0).astype(bf16)
        wide_low = jnp.where(mask_in, dot(low, tile_c), 0.0).astype(bf16)
        return dot(x, wide_high, NT) + dot(x, wide_low, NT)

    raw_re, raw_im = drive(in_re_ref), drive(in_im_ref)
    f_re, f_im = par_ref[2:3, :], par_ref[3:4, :]
    d_re[...] = f_re * raw_re - f_im * raw_im
    d_im[...] = f_re * raw_im + f_im * raw_re
    held = dot(jnp.exp(ret_ref[...]), perm.astype(f32), NT, precision=highest)
    widen = jnp.where(
        iota((groups, gp), 1) // states == iota((groups, gp), 0), 1.0, 0.0
    ).astype(f32)
    shr[...] = dot(held, widen, TN, precision=highest)

    k_re = jnp.broadcast_to(par_ref[0:1, :], (SPANS, gp))
    k_im = jnp.broadcast_to(par_ref[1:2, :], (SPANS, gp))

    def advance(j, s_re, s_im):
        at = pl.ds(pl.multiple_of(j * SPANS, SPANS), SPANS)
        m_re, m_im = cmul(k_re, k_im, s_re, s_im)
        shrink = shr[at, :]
        return at, shrink, shrink * m_re + d_re[at, :], shrink * m_im + d_im[at, :]

    def first(j, state):
        s_re, s_im, total = state
        _, shrink, s_re, s_im = advance(j, s_re, s_im)
        return s_re, s_im, total * shrink

    zero = jnp.zeros((SPANS, gp), f32)
    e_re, e_im, total = lax.fori_loop(0, span, first, (zero, zero, zero + 1.0))
    a_re, a_im = total * par_ref[4:5, :], total * par_ref[5:6, :]

    one = jnp.ones((1, gp), f32)
    nil = jnp.zeros((1, gp), f32)
    c_re, c_im, s_re, s_im = one, nil, nil, nil
    entries = []
    for i in range(SPANS):
        entries.append((c_re, c_im, s_re, s_im))
        ar, ai = a_re[i : i + 1], a_im[i : i + 1]
        s_re, s_im = cmul(ar, ai, s_re, s_im)
        s_re, s_im = s_re + e_re[i : i + 1], s_im + e_im[i : i + 1]
        c_re, c_im = cmul(ar, ai, c_re, c_im)
    for i, part in enumerate((c_re, c_im, s_re, s_im)):
        carry_out[i : i + 1, :] = part

    def carry_copy(k):
        return pltpu.make_async_remote_copy(
            carry_out, carry_in.at[sp], car_s.at[k], car_r.at[k],
            device_id={"sp": lax.rem(sp + k + 1, n_sp)},
        )

    repeat(n_sp - 1, lambda k: carry_copy(k).start())
    c_re, c_im, s_re, s_im = [
        jnp.concatenate([entry[i] for entry in entries], axis=0) for i in range(4)
    ]

    tile_p = jnp.where(
        lax.rem(iota((states, gp), 1), states) == iota((states, gp), 0), 1.0, 0.0
    ).astype(bf16)
    mask_out = iota((chans, gp), 0) // channels == iota((chans, gp), 1) // states

    def wide_out(ref):
        high, low = split(ref[...])
        return [jnp.where(mask_out, dot(part, tile_p), 0.0).astype(bf16) for part in (high, low)]

    o_re, o_im = wide_out(out_re_ref), wide_out(out_im_ref)

    repeat(n_sp - 1, lambda k: carry_copy(k).wait_recv())

    def fold(position, state):
        part = carry_in[position]
        n_re, n_im = cmul(part[0:1], part[1:2], *state)
        return (
            jnp.where(position < sp, n_re + part[2:3], state[0]),
            jnp.where(position < sp, n_im + part[3:4], state[1]),
        )

    state = (nil, nil)
    if n_sp <= 8:
        for position in range(n_sp - 1):
            state = fold(position, state)
    else:
        state = lax.fori_loop(0, n_sp - 1, fold, state)
    m_re, m_im = cmul(c_re, c_im, *state)

    def second(j, state):
        at, _, s_re, s_im = advance(j, *state)
        d_re[at, :] = s_re
        d_im[at, :] = s_im
        return s_re, s_im

    lax.fori_loop(0, span, second, (s_re + m_re, s_im + m_im))

    def read(ref, wide):
        high, low = split(ref[...])
        return dot(high, wide[0], NT) + dot(low, wide[0], NT) + dot(high, wide[1], NT)

    y = read(d_re, o_re) - read(d_im, o_im) + skip_ref[...] * x.astype(f32)
    y = jax.nn.gelu(y).astype(bf16)
    mix_out[...] = dot(perm, y, TN).astype(bf16)

    def mine(index):
        return pl.ds(pl.multiple_of(index * rows, rows), rows)

    mixes = []
    for k in range(n_tp - 1):
        peer = lax.rem(tp + k + 1, n_tp)
        mixes.append(
            pltpu.make_async_remote_copy(
                mix_out.at[mine(peer)], mix_in.at[tp], mix_s.at[k], mix_r.at[k],
                device_id={"tp": peer},
            )
        )
        mixes[-1].start()
    mix_in[tp] = mix_out[mine(tp), :]

    slots = n_sp * cap
    expert_of = iota((rows, slots), 1) // cap
    hit0 = routes_ref[:, 0:1] == expert_of
    hit1 = routes_ref[:, 1:2] == expert_of
    member = jnp.where(hit0 | hit1, 1.0, 0.0)
    lower = jnp.where(iota((rows, rows), 1) < iota((rows, rows), 0), 1.0, 0.0).astype(bf16)
    place = dot(lower, member.astype(bf16))
    wanted = lax.rem(iota((rows, slots), 1), cap).astype(f32)
    chosen = jnp.where(place == wanted, member, 0.0)
    weight = chosen * jnp.where(hit0, rw_ref[:, 0:1], rw_ref[:, 1:2])
    chosen = chosen.astype(bf16)

    for i in range(PROJ_CHUNKS):
        proj_far[i].wait_recv()
        proj_fwd[i].start()
    for copy in mixes:
        copy.wait_recv()
    own.wait()
    proj_near.wait_recv()
    squares = jnp.zeros((rows, 1), f32)
    scaled = []
    for s in range(n_tp):
        part = mix_in[s].astype(f32)
        squares += jnp.sum(part * part, axis=1, keepdims=True)
        scaled.append((part * gain_ref[:, s * chans : (s + 1) * chans]).astype(bf16))
    scale = lax.rsqrt(squares / (n_tp * chans) + 1e-06)
    for copy in proj_fwd:
        copy.wait_recv()
    wide = 256

    def project(i, c):
        cols = pl.ds(pl.multiple_of(i * wide, wide), wide)
        part = dot(scaled[0], proj_all[0, :, cols])
        for s in range(1, n_tp):
            part += dot(scaled[s], proj_all[s, :, cols])
        acc[:, cols] = deep_alpha * res_ref[:, cols].astype(f32) + part * scale
        return c

    lax.fori_loop(0, width // wide, project, 0)
    hid[...] = layer_norm(acc[...], mix_gain_ref[...]).astype(bf16)

    def route_out(i, c):
        cols = pl.ds(pl.multiple_of(i * wide, wide), wide)
        tok_out[:, :, cols] = dot(chosen, hid[:, cols], TN).astype(bf16).reshape(n_sp, cap, wide)
        return c

    lax.fori_loop(0, width // wide, route_out, 0)

    def tok_copy(k):
        peer = lax.rem(sp + k + 1, n_sp)
        return pltpu.make_async_remote_copy(
            tok_out.at[peer], tok_in.at[sp], tok_s.at[k], tok_r.at[k], device_id={"sp": peer}
        )

    repeat(n_sp - 1, lambda k: tok_copy(k).start())
    tok_in[sp] = tok_out[sp]
    for copy in loads[1:]:
        copy.wait()
    repeat(n_sp - 1, lambda k: tok_copy(k).wait_recv())

    arrived = tok_in[...].reshape(slots, width)
    gate = dot(arrived, gate_v[...])
    up = dot(arrived, up_v[...])
    active = (gate * jax.nn.sigmoid(gate) * up).astype(bf16)

    def produce(i, c):
        cols = pl.ds(pl.multiple_of(i * wide, wide), wide)
        ret_out[:, :, cols] = dot(active, down_v[:, cols]).astype(bf16).reshape(n_sp, cap, wide)
        return c

    lax.fori_loop(0, width // wide, produce, 0)

    def back_copy(k):
        peer = lax.rem(sp + k + 1, n_sp)
        return pltpu.make_async_remote_copy(
            ret_out.at[peer], ret_in.at[sp], back_s.at[k], back_r.at[k], device_id={"sp": peer}
        )

    repeat(n_sp - 1, lambda k: back_copy(k).start())
    ret_in[sp] = ret_out[sp]
    w_high, w_low = split(weight)
    repeat(n_sp - 1, lambda k: back_copy(k).wait_recv())

    def combine(i, c):
        cols = pl.ds(pl.multiple_of(i * wide, wide), wide)
        got = ret_in[:, :, cols].reshape(slots, wide)
        acc[:, cols] = (
            deep_alpha * hid[:, cols].astype(f32) + dot(w_high, got) + dot(w_low, got)
        )
        return c

    lax.fori_loop(0, width // wide, combine, 0)
    o_ref[...] = layer_norm(acc[...], final_gain_ref[...]).astype(bf16)

    for copy in proj_far + [proj_near] + proj_fwd + mixes:
        copy.wait_send()
    repeat(n_sp - 1, lambda k: carry_copy(k).wait_send())
    repeat(n_sp - 1, lambda k: tok_copy(k).wait_send())
    repeat(n_sp - 1, lambda k: back_copy(k).wait_send())


def local(
    mixer_input, retention, decay_real, decay_freq, log_step, input_real, input_imag,
    readout_real, readout_imaginary, skip_weight, norm_gain, projection, residual, mix_gain,
    routes, route_weight, expert_gate, expert_up, expert_down, final_gain,
):
    n_sp, n_tp = lax.axis_size("sp"), lax.axis_size("tp")
    tokens, chans = mixer_input.shape
    groups, states, channels = input_real.shape
    gp, rows, width = groups * states, residual.shape[0], residual.shape[1]
    span = tokens // SPANS
    cap = -(-max(2, 2 * rows * PICKS // n_sp) // 16) * 16
    hidden = expert_gate.shape[2]

    stride = jnp.exp(log_step)[:, None]
    growth = decay_real * stride
    turning = decay_freq * stride
    cosine, sine = jnp.cos(turning), jnp.sin(turning)
    size = jnp.exp(growth)
    upper_real = jnp.expm1(growth) * cosine - 2.0 * jnp.sin(0.5 * turning) ** 2
    upper_imag = size * sine
    denominator = decay_real * decay_real + decay_freq * decay_freq
    big = jnp.exp(span * growth)
    params = jnp.stack(
        [
            size * cosine,
            upper_imag,
            (upper_real * decay_real + upper_imag * decay_freq) / denominator,
            (upper_imag * decay_real - upper_real * decay_freq) / denominator,
            big * jnp.cos(span * turning),
            big * jnp.sin(span * turning),
        ]
    ).reshape(6, gp)

    vmem = pl.BlockSpec(memory_space=pltpu.VMEM)
    anywhere = pl.BlockSpec(memory_space=pl.ANY)
    dma = pltpu.SemaphoreType.DMA
    return pl.pallas_call(
        functools.partial(kernel, n_sp, n_tp, groups, channels, states, cap),
        out_shape=jax.ShapeDtypeStruct((rows, width), bf16),
        in_specs=[vmem] * 14 + [anywhere] * 4,
        out_specs=vmem,
        scratch_shapes=[
            pltpu.VMEM((tokens, gp), f32),
            pltpu.VMEM((tokens, gp), f32),
            pltpu.VMEM((tokens, gp), f32),
            pltpu.VMEM((4, gp), f32),
            pltpu.VMEM((n_sp, 4, gp), f32),
            pltpu.VMEM((tokens, chans), bf16),
            pltpu.VMEM((n_tp, rows, chans), bf16),
            pltpu.VMEM((n_tp,) + projection.shape, bf16),
            pltpu.VMEM((width, hidden), bf16),
            pltpu.VMEM((width, hidden), bf16),
            pltpu.VMEM((hidden, width), bf16),
            pltpu.VMEM((rows, width), f32),
            pltpu.VMEM((rows, width), bf16),
            pltpu.VMEM((n_sp, cap, width), bf16),
            pltpu.VMEM((n_sp, cap, width), bf16),
            pltpu.VMEM((n_sp, cap, width), bf16),
            pltpu.VMEM((n_sp, cap, width), bf16),
            dma((4,)),
            dma((n_sp,)), dma((n_sp,)),
            dma((n_tp,)), dma((n_tp,)),
            dma((PROJ_CHUNKS + 1,)), dma((PROJ_CHUNKS + 1,)),
            dma((PROJ_CHUNKS,)), dma((PROJ_CHUNKS,)),
            dma((n_sp,)), dma((n_sp,)),
            dma((n_sp,)), dma((n_sp,)),
        ],
        compiler_params=pltpu.CompilerParams(
            collective_id=0, has_side_effects=True, vmem_limit_bytes=60 * 1024 * 1024
        ),
    )(
        mixer_input, retention, params, skip_weight.reshape(1, chans), norm_gain[None, :],
        input_real.reshape(gp, channels), input_imag.reshape(gp, channels),
        readout_real.reshape(chans, states), readout_imaginary.reshape(chans, states),
        residual, mix_gain[None, :], routes, route_weight, final_gain[None, :],
        projection, expert_gate, expert_up, expert_down,
    )


def solution(mesh):
    in_specs = (
        P("sp", "tp"),
        P("tp", "sp"),
        P("tp", None),
        P("tp", None),
        P("tp"),
        P("tp", None, None),
        P("tp", None, None),
        P("tp", None, None),
        P("tp", None, None),
        P("tp", None),
        P(),
        P("tp", None),
        P(("sp", "tp"), None),
        P(),
        P(("sp", "tp"), None),
        P(("sp", "tp"), None),
        P("sp", None, None),
        P("sp", None, None),
        P("sp", None, None),
        P(),
    )
    out_specs = P(("sp", "tp"), None)
    return jax.shard_map(local, mesh=mesh, in_specs=in_specs, out_specs=out_specs, check_vma=False)
```

profile of v0, /device:TPU:28, one launch (start us, length us, event | category | flops | bytes accessed | tf_op | source)
XLA Modules:
  0.0 101.5 jit_solution(15226346924542215044)
XLA Ops:
  0.0 0.7 exp.9
  0.7 1.4 %reshape.29.skip_ref = f32[1,256]{1,0:T(1,128)} reshape(f32[16,16]{1,0:T(8,128)} %param.29) | data formatting | bytes 2048 | tf_op jit(solution)/shard_map/reshape | solution.py:416
  2.0 1.4 %copy.23.routes_ref = s32[64,2]{1,0:T(8,128)} copy(s32[64,2]{0,1:T(2,128)} %param.34) | data formatting | bytes 1024 | tf_op args[14]
  3.4 1.4 %copy.24.rw_ref = f32[64,2]{1,0:T(8,128)} copy(f32[64,2]{0,1:T(2,128)} %param.35) | data formatting | bytes 1024 | tf_op args[15]
  4.8 0.9 sine_multiply_fusion
  5.7 0.1 stack.26
  5.7 0.1 stack.22
  5.8 0.1 stack.25
  5.9 0.1 stack.21
  6.0 0.1 stack.24
  6.1 0.1 stack.23
  6.1 0.7 stack.27.par_ref
  6.8 1.9 %copy.21 = f32[16,64,16]{2,1,0:T(8,128)} copy(f32[16,64,16]{1,2,0:T(8,128)} %param.25) | data formatting | bytes 131072 | tf_op args[5]
  8.7 1.9 %copy.22 = f32[16,64,16]{2,1,0:T(8,128)} copy(f32[16,64,16]{1,2,0:T(8,128)} %param.26) | data formatting | bytes 131072 | tf_op args[6]
  10.6 89.2 %shard_map.190 = bf16[64,2048]{1,0:T(8,128)(2,1)} custom-call(bf16[256,256]{1,0:T(8,128)(2,1)} %x_ref.1, f32[16,256]{1,0:T(8,128)} %ret_ref.1, f32[6,1024]{1,0:T(8,128)} %stack.27.par_ref, f32[1,256]{1,0:T(1,128)} %reshape.29.skip_ref, f32[1,1024]{1,0:T(1,128)} %bitcast.13, f32[1024,16]{1,0:T(8,128)} %bitcast.7, f32[1024,16]{1,0:T(8,128)} %bitcast.8, ...), custom_call_target="tpu_custom_call" | custom-call | tf_op jit(solution)/shard_map/pallas_call | solution.py:381
  99.8 1.7 %copy.26 = bf16[64,2048]{1,0:T(8,128)(2,1)} copy(bf16[64,2048]{1,0:T(8,128)(2,1)} %shard_map.190) | data formatting | bytes 524288
where the time goes:
time: 102 us; the launch traced here: 101 us
  Pallas kernels  89.2 us (87%)
  local copies, waits for them, and re-layouts  11.4 us (11%)
    pallas_call x1, Pallas kernels, local(): pl.pallas_call(functools.partial(kernel, n_sp, n_tp, groups, channels, st...  89.2 us
    unnamed x5, local copies, waits for them, and re-layouts  8.25 us

commit v1 on v0

--- a/solution.py
+++ b/solution.py
@@ -41,6 +41,13 @@
     return ar * br - ai * bi, ar * bi + ai * br
 
 
+def expm1(value, grown):
+    series = value * 0.125 + 1.0
+    for k in range(7, 1, -1):
+        series = series * value * (1.0 / k) + 1.0
+    return jnp.where(value > -0.4, series * value, grown - 1.0)
+
+
 def repeat(count, body):
     if count <= 8:
         for k in range(count):
@@ -51,12 +58,15 @@
 
 def kernel(
     n_sp, n_tp, groups, channels, states, cap,
-    x_ref, ret_ref, par_ref, skip_ref, gain_ref, in_re_ref, in_im_ref, out_re_ref, out_im_ref,
-    res_ref, mix_gain_ref, routes_ref, rw_ref, final_gain_ref, proj_ref, gate_ref, up_ref, down_ref,
+    x_hbm, ret_hbm, real_hbm, freq_hbm, step_hbm, skip_hbm, gain_hbm, in_re_hbm, in_im_hbm,
+    out_re_hbm, out_im_hbm, res_hbm, mix_gain_hbm, routes_hbm, rw_hbm, final_gain_hbm,
+    proj_ref, gate_ref, up_ref, down_ref,
     o_ref,
+    x_ref, ret_ref, real_ref, freq_ref, step_ref, skip_ref, gain_ref, in_re_ref, in_im_ref,
+    out_re_ref, out_im_ref, res_ref, mix_gain_ref, routes_ref, rw_ref, final_gain_ref,
     d_re, d_im, shr, carry_out, carry_in, mix_out, mix_in, proj_all, gate_v, up_v, down_v,
     acc, hid, tok_out, tok_in, ret_out, ret_in,
-    w_sem, car_s, car_r, mix_s, mix_r, prj_s, prj_r, fwd_s, fwd_r, tok_s, tok_r, back_s, back_r,
+    in_sem, w_sem, car_s, car_r, mix_s, mix_r, prj_s, prj_r, fwd_s, fwd_r, tok_s, tok_r, back_s, back_r,
 ):
     sp, tp = lax.axis_index("sp"), lax.axis_index("tp")
     tokens, chans = x_ref.shape
@@ -65,6 +75,19 @@
     rows = tokens // n_tp
     width = o_ref.shape[1]
 
+    small = (
+        (step_hbm, step_ref), (real_hbm, real_ref), (freq_hbm, freq_ref), (in_re_hbm, in_re_ref),
+        (in_im_hbm, in_im_ref), (x_hbm, x_ref), (ret_hbm, ret_ref), (skip_hbm, skip_ref),
+        (out_re_hbm, out_re_ref), (out_im_hbm, out_im_ref), (gain_hbm, gain_ref),
+        (routes_hbm, routes_ref), (rw_hbm, rw_ref), (res_hbm, res_ref),
+        (mix_gain_hbm, mix_gain_ref), (final_gain_hbm, final_gain_ref),
+    )
+    fetches = [
+        pltpu.make_async_copy(src, dst, in_sem.at[i]) for i, (src, dst) in enumerate(small)
+    ]
+    for fetch in fetches:
+        fetch.start()
+
     barrier = pltpu.get_barrier_semaphore()
 
     def greet_sp(k):
@@ -113,34 +136,63 @@
         copy.start()
     proj_near.start()
 
+    for fetch in fetches:
+        fetch.wait()
+
+    eye = iota((groups, groups), 0) == iota((groups, groups), 1)
+    stride = jnp.exp(jnp.sum(jnp.where(eye, step_ref[...], 0.0), axis=1, keepdims=True))
+    real, freq = real_ref[...], freq_ref[...]
+    growth, turning = real * stride, freq * stride
+    cosine, sine, half = jnp.cos(turning), jnp.sin(turning), jnp.sin(0.5 * turning)
+    size = jnp.exp(growth)
+    upper_real = expm1(growth, size) * cosine - 2.0 * half * half
+    keep_re, upper_imag = size * cosine, size * sine
+    denominator = real * real + freq * freq
+    f_re = (upper_real * real + upper_imag * freq) / denominator
+    f_im = (upper_imag * real - upper_real * freq) / denominator
+    big_re, big_im = keep_re, upper_imag
+    for _ in range(span.bit_length() - 1):
+        big_re, big_im = cmul(big_re, big_im, big_re, big_im)
+
+    tile_p = jnp.where(
+        lax.rem(iota((states, gp), 1), states) == iota((states, gp), 0), 1.0, 0.0
+    )
+    widen = jnp.where(
+        iota((groups, gp), 1) // states == iota((groups, gp), 0), 1.0, 0.0
+    ).astype(f32)
+    packed = jnp.concatenate([keep_re, upper_imag, big_re, big_im], axis=0)
+    spread = dot(packed, tile_p, precision=highest)
+    k_re, k_im, b_re, b_im = [
+        jnp.sum(spread[i * groups : (i + 1) * groups] * widen, axis=0, keepdims=True)
+        for i in range(4)
+    ]
+    tile_p = tile_p.astype(bf16)
+    mask_out = iota((chans, gp), 0) // channels == iota((chans, gp), 1) // states
+
+    def wide(value):
+        return [
+            jnp.where(mask_out, dot(part, tile_p), 0.0).astype(bf16) for part in split(value)
+        ]
+
+    copies = jnp.where(
+        iota((chans, groups), 0) // channels == iota((chans, groups), 1), 1.0, 0.0
+    ).astype(f32)
+    f_re, f_im = dot(copies, f_re, precision=highest), dot(copies, f_im, precision=highest)
+    bar_re, bar_im = cmul(f_re, f_im, in_re_ref[...], in_im_ref[...])
+
     row_i, col_i = iota((tokens, tokens), 0), iota((tokens, tokens), 1)
     perm = jnp.where(
         col_i == lax.rem(row_i, SPANS) * span + row_i // SPANS, 1.0, 0.0
     ).astype(bf16)
     x = dot(perm, x_ref[...]).astype(bf16)
-    tile_c = jnp.where(
-        lax.rem(iota((channels, chans), 1), channels) == iota((channels, chans), 0), 1.0, 0.0
-    ).astype(bf16)
-    mask_in = iota((gp, chans), 0) // states == iota((gp, chans), 1) // channels
-
-    def drive(ref):
-        high, low = split(ref[...])
-        wide_high = jnp.where(mask_in, dot(high, tile_c), 0.0).astype(bf16)
-        wide_low = jnp.where(mask_in, dot(low, tile_c), 0.0).astype(bf16)
-        return dot(x, wide_high, NT) + dot(x, wide_low, NT)
-
-    raw_re, raw_im = drive(in_re_ref), drive(in_im_ref)
-    f_re, f_im = par_ref[2:3, :], par_ref[3:4, :]
-    d_re[...] = f_re * raw_re - f_im * raw_im
-    d_im[...] = f_re * raw_im + f_im * raw_re
+    for bar, d_ref in ((bar_re, d_re), (bar_im, d_im)):
+        high, low = wide(bar)
+        d_ref[...] = dot(x, high) + dot(x, low)
     held = dot(jnp.exp(ret_ref[...]), perm.astype(f32), NT, precision=highest)
-    widen = jnp.where(
-        iota((groups, gp), 1) // states == iota((groups, gp), 0), 1.0, 0.0
-    ).astype(f32)
     shr[...] = dot(held, widen, TN, precision=highest)
 
-    k_re = jnp.broadcast_to(par_ref[0:1, :], (SPANS, gp))
-    k_im = jnp.broadcast_to(par_ref[1:2, :], (SPANS, gp))
+    k_re = jnp.broadcast_to(k_re, (SPANS, gp))
+    k_im = jnp.broadcast_to(k_im, (SPANS, gp))
 
     def advance(j, s_re, s_im):
         at = pl.ds(pl.multiple_of(j * SPANS, SPANS), SPANS)
@@ -155,7 +207,7 @@
 
     zero = jnp.zeros((SPANS, gp), f32)
     e_re, e_im, total = lax.fori_loop(0, span, first, (zero, zero, zero + 1.0))
-    a_re, a_im = total * par_ref[4:5, :], total * par_ref[5:6, :]
+    a_re, a_im = total * b_re, total * b_im
 
     one = jnp.ones((1, gp), f32)
     nil = jnp.zeros((1, gp), f32)
@@ -181,16 +233,13 @@
         jnp.concatenate([entry[i] for entry in entries], axis=0) for i in range(4)
     ]
 
-    tile_p = jnp.where(
-        lax.rem(iota((states, gp), 1), states) == iota((states, gp), 0), 1.0, 0.0
-    ).astype(bf16)
-    mask_out = iota((chans, gp), 0) // channels == iota((chans, gp), 1) // states
-
-    def wide_out(ref):
-        high, low = split(ref[...])
-        return [jnp.where(mask_out, dot(part, tile_p), 0.0).astype(bf16) for part in (high, low)]
-
-    o_re, o_im = wide_out(out_re_ref), wide_out(out_im_ref)
+    o_re, o_im = wide(out_re_ref[...]), wide(out_im_ref[...])
+    tile_c = jnp.where(
+        lax.rem(iota((channels, chans), 1), channels) == iota((channels, chans), 0), 1.0, 0.0
+    ).astype(f32)
+    own_group = iota((groups, chans), 1) // channels == iota((groups, chans), 0)
+    skip = jnp.where(own_group, dot(skip_ref[...], tile_c, precision=highest), 0.0)
+    skip = jnp.sum(skip, axis=0, keepdims=True)
 
     repeat(n_sp - 1, lambda k: carry_copy(k).wait_recv())
 
@@ -222,7 +271,7 @@
         high, low = split(ref[...])
         return dot(high, wide[0], NT) + dot(low, wide[0], NT) + dot(high, wide[1], NT)
 
-    y = read(d_re, o_re) - read(d_im, o_im) + skip_ref[...] * x.astype(f32)
+    y = read(d_re, o_re) - read(d_im, o_im) + skip * x.astype(f32)
     y = jax.nn.gelu(y).astype(bf16)
     mix_out[...] = dot(perm, y, TN).astype(bf16)
 
@@ -242,15 +291,15 @@
     mix_in[tp] = mix_out[mine(tp), :]
 
     slots = n_sp * cap
-    expert_of = iota((rows, slots), 1) // cap
-    hit0 = routes_ref[:, 0:1] == expert_of
-    hit1 = routes_ref[:, 1:2] == expert_of
+    expert_of = iota((slots, rows), 0) // cap
+    hit0 = routes_ref[0:1, :] == expert_of
+    hit1 = routes_ref[1:2, :] == expert_of
     member = jnp.where(hit0 | hit1, 1.0, 0.0)
-    lower = jnp.where(iota((rows, rows), 1) < iota((rows, rows), 0), 1.0, 0.0).astype(bf16)
-    place = dot(lower, member.astype(bf16))
-    wanted = lax.rem(iota((rows, slots), 1), cap).astype(f32)
+    upper = jnp.where(iota((rows, rows), 0) < iota((rows, rows), 1), 1.0, 0.0).astype(bf16)
+    place = dot(member.astype(bf16), upper)
+    wanted = lax.rem(iota((slots, rows), 0), cap).astype(f32)
     chosen = jnp.where(place == wanted, member, 0.0)
-    weight = chosen * jnp.where(hit0, rw_ref[:, 0:1], rw_ref[:, 1:2])
+    weight = chosen * jnp.where(hit0, rw_ref[0:1, :], rw_ref[1:2, :])
     chosen = chosen.astype(bf16)
 
     for i in range(PROJ_CHUNKS):
@@ -284,7 +333,7 @@
 
     def route_out(i, c):
         cols = pl.ds(pl.multiple_of(i * wide, wide), wide)
-        tok_out[:, :, cols] = dot(chosen, hid[:, cols], TN).astype(bf16).reshape(n_sp, cap, wide)
+        tok_out[:, :, cols] = dot(chosen, hid[:, cols]).astype(bf16).reshape(n_sp, cap, wide)
         return c
 
     lax.fori_loop(0, width // wide, route_out, 0)
@@ -328,7 +377,7 @@
         cols = pl.ds(pl.multiple_of(i * wide, wide), wide)
         got = ret_in[:, :, cols].reshape(slots, wide)
         acc[:, cols] = (
-            deep_alpha * hid[:, cols].astype(f32) + dot(w_high, got) + dot(w_low, got)
+            deep_alpha * hid[:, cols].astype(f32) + dot(w_high, got, TN) + dot(w_low, got, TN)
         )
         return c
 
@@ -351,39 +400,28 @@
     tokens, chans = mixer_input.shape
     groups, states, channels = input_real.shape
     gp, rows, width = groups * states, residual.shape[0], residual.shape[1]
-    span = tokens // SPANS
     cap = -(-max(2, 2 * rows * PICKS // n_sp) // 16) * 16
     hidden = expert_gate.shape[2]
 
-    stride = jnp.exp(log_step)[:, None]
-    growth = decay_real * stride
-    turning = decay_freq * stride
-    cosine, sine = jnp.cos(turning), jnp.sin(turning)
-    size = jnp.exp(growth)
-    upper_real = jnp.expm1(growth) * cosine - 2.0 * jnp.sin(0.5 * turning) ** 2
-    upper_imag = size * sine
-    denominator = decay_real * decay_real + decay_freq * decay_freq
-    big = jnp.exp(span * growth)
-    params = jnp.stack(
-        [
-            size * cosine,
-            upper_imag,
-            (upper_real * decay_real + upper_imag * decay_freq) / denominator,
-            (upper_imag * decay_real - upper_real * decay_freq) / denominator,
-            big * jnp.cos(span * turning),
-            big * jnp.sin(span * turning),
-        ]
-    ).reshape(6, gp)
-
+    def compact(value):
+        return jnp.swapaxes(value, 1, 2).reshape(chans, states)
+
+    small = (
+        mixer_input, retention, decay_real, decay_freq, log_step[None, :], skip_weight,
+        norm_gain[None, :], compact(input_real), compact(input_imag),
+        readout_real.reshape(chans, states), readout_imaginary.reshape(chans, states),
+        residual, mix_gain[None, :], routes.T, route_weight.T, final_gain[None, :],
+    )
     vmem = pl.BlockSpec(memory_space=pltpu.VMEM)
     anywhere = pl.BlockSpec(memory_space=pl.ANY)
     dma = pltpu.SemaphoreType.DMA
     return pl.pallas_call(
         functools.partial(kernel, n_sp, n_tp, groups, channels, states, cap),
         out_shape=jax.ShapeDtypeStruct((rows, width), bf16),
-        in_specs=[vmem] * 14 + [anywhere] * 4,
+        in_specs=[anywhere] * (len(small) + 4),
         out_specs=vmem,
-        scratch_shapes=[
+        scratch_shapes=[pltpu.VMEM(value.shape, value.dtype) for value in small]
+        + [
             pltpu.VMEM((tokens, gp), f32),
             pltpu.VMEM((tokens, gp), f32),
             pltpu.VMEM((tokens, gp), f32),
@@ -401,7 +439,7 @@
             pltpu.VMEM((n_sp, cap, width), bf16),
             pltpu.VMEM((n_sp, cap, width), bf16),
             pltpu.VMEM((n_sp, cap, width), bf16),
-            dma((4,)),
+            dma((len(small),)), dma((4,)),
             dma((n_sp,)), dma((n_sp,)),
             dma((n_tp,)), dma((n_tp,)),
             dma((PROJ_CHUNKS + 1,)), dma((PROJ_CHUNKS + 1,)),
@@ -413,10 +451,7 @@
             collective_id=0, has_side_effects=True, vmem_limit_bytes=60 * 1024 * 1024
         ),
     )(
-        mixer_input, retention, params, skip_weight.reshape(1, chans), norm_gain[None, :],
-        input_real.reshape(gp, channels), input_imag.reshape(gp, channels),
-        readout_real.reshape(chans, states), readout_imaginary.reshape(chans, states),
-        residual, mix_gain[None, :], routes, route_weight, final_gain[None, :],
+        *small,
         projection, expert_gate, expert_up, expert_down,
     )
 

time: 102 us -> 89.5 us (0.88)
  local copies, waits for them, and re-layouts: 11.4 us -> 1.67 us
  Pallas kernels: 89.2 us -> 87.7 us
    unnamed x5 -> x1, local copies, waits for them, and re-layouts: 8.25 us -> 1.67 us
    pallas_call x1, Pallas kernels: 89.2 us -> 87.7 us  [local(): pl.pallas_call(functools.partial(kernel, n_sp, n_tp, groups, channels, st...]
    reshape x1 -> x0, local copies, waits for them, and re-layouts: 1.36 us -> none  [local(): skip_weight.reshape(1, chans)]
    another operation x7 -> x0, local copies, waits for them, and re-layouts: 1.12 us -> none  [local(): jnp.stack([size * cosine, upper_imag, (upper_real * decay_real + upper_im...]
where the time goes in v1:
time: 89.5 us; the launch traced here: 89.4 us
  Pallas kernels  87.7 us (98%)
  local copies, waits for them, and re-layouts  1.67 us (2%)
    pallas_call x1, Pallas kernels, local(): pl.pallas_call(functools.partial(kernel, n_sp, n_tp, groups, channels, st...  87.7 us

profile of v1, /device:TPU:28, one launch (start us, length us, event | category | flops | bytes accessed | tf_op | source)
XLA Modules:
  0.0 89.4 jit_solution(11815116835025850021)
XLA Ops:
  0.0 87.7 %shard_map.190 = bf16[64,2048]{1,0:T(8,128)(2,1)} custom-call(bf16[256,256]{1,0:T(8,128)(2,1)} %x_hbm.1, f32[16,256]{1,0:T(8,128)} %ret_hbm.1, f32[16,64]{1,0:T(8,128)} %real_hbm.1, f32[16,64]{1,0:T(8,128)} %freq_hbm.1, f32[1,16]{1,0:T(1,128)} %bitcast.23, f32[16,16]{1,0:T(8,128)} %skip_hbm.1, f32[1,1024]{1,0:T(1,128)} %bitcast.20, f32[256,64]{1,0:T(8,128)} %bitcast.14, ...), custom_call_target="tpu_custom_call" | custom-call | tf_op jit(solution)/shard_map/pallas_call | solution.py:418
  87.7 1.7 %copy.22 = bf16[64,2048]{1,0:T(8,128)(2,1)} copy(bf16[64,2048]{1,0:T(8,128)(2,1)} %shard_map.190) | data formatting | bytes 524288

commit v2 on v1

--- a/solution.py
+++ b/solution.py
@@ -14,7 +14,11 @@
 highest = lax.Precision.HIGHEST
 NT = (((1,), (1,)), ((), ()))
 TN = (((0,), (0,)), ((), ()))
-PROJ_CHUNKS = 4
+PROJ_CHUNKS = 8
+PROJ_FIRST = 3
+LO = 2
+HALVES = 2
+BATCH_ROWS = 128
 
 
 def dot(a, b, dims=None, precision=None):
@@ -65,8 +69,10 @@
     x_ref, ret_ref, real_ref, freq_ref, step_ref, skip_ref, gain_ref, in_re_ref, in_im_ref,
     out_re_ref, out_im_ref, res_ref, mix_gain_ref, routes_ref, rw_ref, final_gain_ref,
     d_re, d_im, shr, carry_out, carry_in, mix_out, mix_in, proj_all, gate_v, up_v, down_v,
-    acc, hid, tok_out, tok_in, ret_out, ret_in,
-    in_sem, w_sem, car_s, car_r, mix_s, mix_r, prj_s, prj_r, fwd_s, fwd_r, tok_s, tok_r, back_s, back_r,
+    acc, hid, scaled_v, acc_b, hid_b, pick_out, pick_in, raw, res_out, res_in, y_out, y_in,
+    ret_out, ret_in,
+    in_sem, w_sem, car_s, car_r, mix_s, mix_r, prj_s, prj_r, fwd_s, fwd_r,
+    pick_s, pick_r, up_s, up_r, low_s, low_r, res_s, res_r, y_s, y_r, back_s, back_r,
 ):
     sp, tp = lax.axis_index("sp"), lax.axis_index("tp")
     tokens, chans = x_ref.shape
@@ -132,12 +138,125 @@
         )
         for i in range(PROJ_CHUNKS)
     ]
-    for copy in proj_far:
+    for copy in proj_far[:PROJ_FIRST]:
         copy.start()
     proj_near.start()
 
     for fetch in fetches:
         fetch.wait()
+
+    slots = n_sp * cap
+    expert_of = iota((slots, rows), 0) // cap
+    hit0 = routes_ref[0:1, :] == expert_of
+    hit1 = routes_ref[1:2, :] == expert_of
+    member = jnp.where(hit0 | hit1, 1.0, 0.0)
+    upper = jnp.where(iota((rows, rows), 0) < iota((rows, rows), 1), 1.0, 0.0).astype(bf16)
+    place = dot(member.astype(bf16), upper)
+    wanted = lax.rem(iota((slots, rows), 0), cap).astype(f32)
+    chosen = jnp.where(place == wanted, member, 0.0)
+    weight = chosen * jnp.where(hit0, rw_ref[0:1, :], rw_ref[1:2, :])
+    chosen = chosen.astype(bf16)
+    w_high, w_low = split(weight)
+
+    def every(count, width, body):
+        def step(i, c):
+            body(pl.ds(pl.multiple_of(i * width, width), width))
+            return c
+
+        lax.fori_loop(0, count // width, step, 0)
+
+    hi, lo = sp // LO, lax.rem(sp, LO)
+    line = n_sp // LO
+    flood = n_sp <= 8
+    piece_rows = rows // HALVES
+
+    def pick_copy(k):
+        peer = lax.rem(hi + k + 1, line)
+        return pltpu.make_async_remote_copy(
+            pick_out.at[pl.ds(pl.multiple_of(peer * LO * cap, LO * cap), LO * cap)],
+            pick_in.at[hi], pick_s.at[k], pick_r.at[k], device_id={"sp": peer * LO + lo},
+        )
+
+    def hop(sign, step, part):
+        owner = lax.rem(hi - sign * step + line, line)
+        piece = pl.ds(part * piece_rows, piece_rows)
+        source = res_ref.at[piece] if step == 0 else raw.at[owner, piece]
+        s_sem, r_sem = (up_s, up_r) if sign > 0 else (low_s, low_r)
+        at = step * HALVES + part
+        return pltpu.make_async_remote_copy(
+            source, raw.at[owner, piece], s_sem.at[at], r_sem.at[at],
+            device_id={"sp": lax.rem(sp + sign * LO + n_sp, n_sp)},
+        )
+
+    def inside(value):
+        return (value >= 0) & (value < line)
+
+    def hop_start(step, part):
+        for sign in (1, -1):
+            @pl.when(inside(hi - sign * step) & inside(hi + sign))
+            def _():
+                hop(sign, step, part).start()
+
+    def hop_sent(step, part):
+        for sign in (1, -1):
+            @pl.when(inside(hi - sign * step) & inside(hi + sign))
+            def _():
+                hop(sign, step, part).wait_send()
+
+    def hop_pass(step, part):
+        for sign in (1, -1):
+            @pl.when(inside(hi - sign * (step + 1)))
+            def _():
+                owner = lax.rem(hi - sign * (step + 1) + line, line)
+                piece = pl.ds(part * piece_rows, piece_rows)
+                s_sem, r_sem = (up_s, up_r) if sign > 0 else (low_s, low_r)
+                at = step * HALVES + part
+                pltpu.make_async_remote_copy(
+                    raw.at[owner, piece], raw.at[owner, piece], s_sem.at[at], r_sem.at[at],
+                    device_id={"sp": lax.rem(sp + LO, n_sp)},
+                ).wait_recv()
+        if step + 1 < line - 1:
+            hop_start(step + 1, part)
+
+    def res_copy(owner):
+        return pltpu.make_async_remote_copy(
+            res_out.at[owner * LO + 1 - lo], res_in.at[owner * LO + lo],
+            res_s.at[owner], res_r.at[owner], device_id={"sp": hi * LO + 1 - lo},
+        )
+
+    def share(owner, pick, rows_of):
+        def step(cols):
+            both = dot(pick, rows_of[:, cols]).astype(bf16).reshape(LO, cap, 256)
+            res_out[pl.ds(owner * LO, LO), :, cols] = both
+
+        every(width, 256, step)
+        res_in[owner * LO + lo] = res_out[owner * LO + lo]
+        res_copy(owner).start()
+
+    def share_line(step):
+        for sign in (1, -1):
+            @pl.when(inside(hi - sign * step))
+            def _():
+                owner = lax.rem(hi - sign * step + line, line)
+                share(owner, pick_in[owner], raw.at[owner])
+
+    def send_res(k):
+        peer = lax.rem(sp + k + 1, n_sp)
+        return pltpu.make_async_remote_copy(
+            res_out.at[peer], res_in.at[sp], res_s.at[k], res_r.at[k], device_id={"sp": peer}
+        )
+
+    pick_out[...] = chosen
+    if flood:
+        repeat(line - 1, lambda k: pick_copy(k).start())
+        hop_start(0, 0)
+    else:
+        def spread_res(cols):
+            res_out[:, :, cols] = dot(chosen, res_ref[:, cols]).astype(bf16).reshape(n_sp, cap, 256)
+
+        every(width, 256, spread_res)
+        res_in[sp] = res_out[sp]
+        repeat(n_sp - 1, lambda k: send_res(k).start())
 
     eye = iota((groups, groups), 0) == iota((groups, groups), 1)
     stride = jnp.exp(jnp.sum(jnp.where(eye, step_ref[...], 0.0), axis=1, keepdims=True))
@@ -153,6 +272,9 @@
     big_re, big_im = keep_re, upper_imag
     for _ in range(span.bit_length() - 1):
         big_re, big_im = cmul(big_re, big_im, big_re, big_im)
+    full_re, full_im = big_re, big_im
+    for _ in range(SPANS.bit_length() - 1):
+        full_re, full_im = cmul(full_re, full_im, full_re, full_im)
 
     tile_p = jnp.where(
         lax.rem(iota((states, gp), 1), states) == iota((states, gp), 0), 1.0, 0.0
@@ -160,11 +282,11 @@
     widen = jnp.where(
         iota((groups, gp), 1) // states == iota((groups, gp), 0), 1.0, 0.0
     ).astype(f32)
-    packed = jnp.concatenate([keep_re, upper_imag, big_re, big_im], axis=0)
+    packed = jnp.concatenate([keep_re, upper_imag, big_re, big_im, full_re, full_im], axis=0)
     spread = dot(packed, tile_p, precision=highest)
-    k_re, k_im, b_re, b_im = [
+    k_re, k_im, b_re, b_im, full_re, full_im = [
         jnp.sum(spread[i * groups : (i + 1) * groups] * widen, axis=0, keepdims=True)
-        for i in range(4)
+        for i in range(6)
     ]
     tile_p = tile_p.astype(bf16)
     mask_out = iota((chans, gp), 0) // channels == iota((chans, gp), 1) // states
@@ -219,7 +341,10 @@
         s_re, s_im = cmul(ar, ai, s_re, s_im)
         s_re, s_im = s_re + e_re[i : i + 1], s_im + e_im[i : i + 1]
         c_re, c_im = cmul(ar, ai, c_re, c_im)
-    for i, part in enumerate((c_re, c_im, s_re, s_im)):
+    held_all = total[0:1]
+    for i in range(1, SPANS):
+        held_all = held_all * total[i : i + 1]
+    for i, part in enumerate((held_all, s_re, s_im)):
         carry_out[i : i + 1, :] = part
 
     def carry_copy(k):
@@ -228,7 +353,25 @@
             device_id={"sp": lax.rem(sp + k + 1, n_sp)},
         )
 
-    repeat(n_sp - 1, lambda k: carry_copy(k).start())
+    def carry_start(k):
+        @pl.when(sp + k + 1 < n_sp)
+        def _():
+            carry_copy(k).start()
+
+    def carry_arrived(k):
+        @pl.when(sp > k)
+        def _():
+            carry_copy(k).wait_recv()
+
+    def carry_sent(k):
+        @pl.when(sp + k + 1 < n_sp)
+        def _():
+            carry_copy(k).wait_send()
+
+    repeat(n_sp - 1, carry_start)
+    if flood:
+        for part in range(1, HALVES):
+            hop_start(0, part)
     c_re, c_im, s_re, s_im = [
         jnp.concatenate([entry[i] for entry in entries], axis=0) for i in range(4)
     ]
@@ -241,14 +384,20 @@
     skip = jnp.where(own_group, dot(skip_ref[...], tile_c, precision=highest), 0.0)
     skip = jnp.sum(skip, axis=0, keepdims=True)
 
-    repeat(n_sp - 1, lambda k: carry_copy(k).wait_recv())
+    if flood:
+        share(hi, pick_out[pl.ds(pl.multiple_of(hi * LO * cap, LO * cap), LO * cap), :], res_ref)
+        hop_pass(0, 0)
+    repeat(n_sp - 1, carry_arrived)
+    if flood:
+        for part in range(1, HALVES):
+            hop_pass(0, part)
 
     def fold(position, state):
         part = carry_in[position]
-        n_re, n_im = cmul(part[0:1], part[1:2], *state)
+        n_re, n_im = cmul(part[0:1] * full_re, part[0:1] * full_im, *state)
         return (
-            jnp.where(position < sp, n_re + part[2:3], state[0]),
-            jnp.where(position < sp, n_im + part[3:4], state[1]),
+            jnp.where(position < sp, n_re + part[1:2], state[0]),
+            jnp.where(position < sp, n_im + part[2:3], state[1]),
         )
 
     state = (nil, nil)
@@ -288,107 +437,139 @@
             )
         )
         mixes[-1].start()
+    for copy in proj_far[PROJ_FIRST:]:
+        copy.start()
     mix_in[tp] = mix_out[mine(tp), :]
-
-    slots = n_sp * cap
-    expert_of = iota((slots, rows), 0) // cap
-    hit0 = routes_ref[0:1, :] == expert_of
-    hit1 = routes_ref[1:2, :] == expert_of
-    member = jnp.where(hit0 | hit1, 1.0, 0.0)
-    upper = jnp.where(iota((rows, rows), 0) < iota((rows, rows), 1), 1.0, 0.0).astype(bf16)
-    place = dot(member.astype(bf16), upper)
-    wanted = lax.rem(iota((slots, rows), 0), cap).astype(f32)
-    chosen = jnp.where(place == wanted, member, 0.0)
-    weight = chosen * jnp.where(hit0, rw_ref[0:1, :], rw_ref[1:2, :])
-    chosen = chosen.astype(bf16)
-
+    if flood:
+        repeat(line - 1, lambda k: pick_copy(k).wait_recv())
+        hop_pass(1, 0)
+        share_line(1)
+    for copy in mixes:
+        copy.wait_recv()
+
+    total_chans = n_tp * chans
+    for part in range(n_tp):
+        y_out[:, :, part * chans : (part + 1) * chans] = (
+            dot(chosen, mix_in[part]).astype(bf16).reshape(n_sp, cap, chans)
+        )
+
+    take = BATCH_ROWS // cap
+    batches = n_sp // take
+    home = sp // take
+
+    def batch_of(i):
+        return lax.rem(home + batches // 2 + i, batches) if batches > 1 else 0
+
+    def others(i, body):
+        base = batch_of(i) * take
+
+        def one(j):
+            peer = base + j
+
+            @pl.when(peer != sp)
+            def _():
+                body(peer)
+
+        repeat(take, one)
+
+    def y_copy(peer, source):
+        return pltpu.make_async_remote_copy(
+            y_out.at[peer], y_in.at[source], y_s.at[peer], y_r.at[source], device_id={"sp": peer}
+        )
+
+    repeat(batches, lambda i: others(i, lambda peer: y_copy(peer, sp).start()))
+    y_in[sp] = y_out[sp]
+
+    if flood:
+        for part in range(1, HALVES):
+            hop_pass(1, part)
+        share_line(2)
+        for step in range(2, line - 1):
+            for part in range(HALVES):
+                hop_pass(step, part)
+            share_line(step + 1)
     for i in range(PROJ_CHUNKS):
         proj_far[i].wait_recv()
         proj_fwd[i].start()
-    for copy in mixes:
-        copy.wait_recv()
     own.wait()
     proj_near.wait_recv()
-    squares = jnp.zeros((rows, 1), f32)
-    scaled = []
-    for s in range(n_tp):
-        part = mix_in[s].astype(f32)
-        squares += jnp.sum(part * part, axis=1, keepdims=True)
-        scaled.append((part * gain_ref[:, s * chans : (s + 1) * chans]).astype(bf16))
-    scale = lax.rsqrt(squares / (n_tp * chans) + 1e-06)
     for copy in proj_fwd:
         copy.wait_recv()
-    wide = 256
-
-    def project(i, c):
-        cols = pl.ds(pl.multiple_of(i * wide, wide), wide)
-        part = dot(scaled[0], proj_all[0, :, cols])
-        for s in range(1, n_tp):
-            part += dot(scaled[s], proj_all[s, :, cols])
-        acc[:, cols] = deep_alpha * res_ref[:, cols].astype(f32) + part * scale
-        return c
-
-    lax.fori_loop(0, width // wide, project, 0)
-    hid[...] = layer_norm(acc[...], mix_gain_ref[...]).astype(bf16)
-
-    def route_out(i, c):
-        cols = pl.ds(pl.multiple_of(i * wide, wide), wide)
-        tok_out[:, :, cols] = dot(chosen, hid[:, cols]).astype(bf16).reshape(n_sp, cap, wide)
-        return c
-
-    lax.fori_loop(0, width // wide, route_out, 0)
-
-    def tok_copy(k):
-        peer = lax.rem(sp + k + 1, n_sp)
-        return pltpu.make_async_remote_copy(
-            tok_out.at[peer], tok_in.at[sp], tok_s.at[k], tok_r.at[k], device_id={"sp": peer}
-        )
-
-    repeat(n_sp - 1, lambda k: tok_copy(k).start())
-    tok_in[sp] = tok_out[sp]
+    if flood:
+        for owner in range(line):
+            res_copy(owner).wait_recv()
+    else:
+        repeat(n_sp - 1, lambda k: send_res(k).wait_recv())
     for copy in loads[1:]:
         copy.wait()
-    repeat(n_sp - 1, lambda k: tok_copy(k).wait_recv())
-
-    arrived = tok_in[...].reshape(slots, width)
-    gate = dot(arrived, gate_v[...])
-    up = dot(arrived, up_v[...])
-    active = (gate * jax.nn.sigmoid(gate) * up).astype(bf16)
-
-    def produce(i, c):
-        cols = pl.ds(pl.multiple_of(i * wide, wide), wide)
-        ret_out[:, :, cols] = dot(active, down_v[:, cols]).astype(bf16).reshape(n_sp, cap, wide)
-        return c
-
-    lax.fori_loop(0, width // wide, produce, 0)
-
-    def back_copy(k):
-        peer = lax.rem(sp + k + 1, n_sp)
+
+    def hidden_of(y, scaled_ref, acc_ref, residual_of):
+        squares = jnp.sum(y * y, axis=1, keepdims=True)
+        scaled_ref[...] = (y * gain_ref[...]).astype(bf16)
+        scale = lax.rsqrt(squares / total_chans + 1e-06)
+
+        def project(cols):
+            weights = proj_all[:, :, cols].reshape(total_chans, 256)
+            part = dot(scaled_ref[...], weights)
+            acc_ref[:, cols] = deep_alpha * residual_of(cols).astype(f32) + part * scale
+
+        every(width, 256, project)
+        return layer_norm(acc_ref[...], mix_gain_ref[...]).astype(bf16)
+
+    def back_copy(peer, source):
         return pltpu.make_async_remote_copy(
-            ret_out.at[peer], ret_in.at[sp], back_s.at[k], back_r.at[k], device_id={"sp": peer}
-        )
-
-    repeat(n_sp - 1, lambda k: back_copy(k).start())
+            ret_out.at[peer], ret_in.at[source], back_s.at[peer], back_r.at[source],
+            device_id={"sp": peer},
+        )
+
+    def expert(i):
+        base = batch_of(i) * take
+        these = pl.ds(base, take)
+        others(i, lambda peer: y_copy(peer, peer).wait_recv())
+        y = y_in[these].reshape(BATCH_ROWS, total_chans).astype(f32)
+        hid_b[...] = hidden_of(
+            y, scaled_v, acc_b, lambda cols: res_in[these, :, cols].reshape(BATCH_ROWS, 256)
+        )
+        gate, up = dot(hid_b[...], gate_v[...]), dot(hid_b[...], up_v[...])
+        active = (gate * jax.nn.sigmoid(gate) * up).astype(bf16)
+
+        def produce(cols):
+            ret_out[these, :, cols] = (
+                dot(active, down_v[:, cols]).astype(bf16).reshape(take, cap, 256)
+            )
+
+        every(width, 256, produce)
+        others(i, lambda peer: back_copy(peer, sp).start())
+
+    repeat(batches, expert)
     ret_in[sp] = ret_out[sp]
-    w_high, w_low = split(weight)
-    repeat(n_sp - 1, lambda k: back_copy(k).wait_recv())
-
-    def combine(i, c):
-        cols = pl.ds(pl.multiple_of(i * wide, wide), wide)
-        got = ret_in[:, :, cols].reshape(slots, wide)
+    y = jnp.concatenate([mix_in[part].astype(f32) for part in range(n_tp)], axis=1)
+    hid[...] = hidden_of(y, scaled_v.at[pl.ds(0, rows)], acc, lambda cols: res_ref[:, cols])
+    repeat(batches, lambda i: others(i, lambda peer: back_copy(peer, peer).wait_recv()))
+
+    def combine(cols):
+        got = ret_in[:, :, cols].reshape(slots, 256)
         acc[:, cols] = (
             deep_alpha * hid[:, cols].astype(f32) + dot(w_high, got, TN) + dot(w_low, got, TN)
         )
-        return c
-
-    lax.fori_loop(0, width // wide, combine, 0)
+
+    every(width, 256, combine)
     o_ref[...] = layer_norm(acc[...], final_gain_ref[...]).astype(bf16)
 
     for copy in proj_far + [proj_near] + proj_fwd + mixes:
         copy.wait_send()
-    repeat(n_sp - 1, lambda k: carry_copy(k).wait_send())
-    repeat(n_sp - 1, lambda k: tok_copy(k).wait_send())
-    repeat(n_sp - 1, lambda k: back_copy(k).wait_send())
+    repeat(n_sp - 1, carry_sent)
+    if flood:
+        repeat(line - 1, lambda k: pick_copy(k).wait_send())
+        for step in range(line - 1):
+            for part in range(HALVES):
+                hop_sent(step, part)
+        for owner in range(line):
+            res_copy(owner).wait_send()
+    else:
+        repeat(n_sp - 1, lambda k: send_res(k).wait_send())
+    repeat(batches, lambda i: others(i, lambda peer: y_copy(peer, sp).wait_send()))
+    repeat(batches, lambda i: others(i, lambda peer: back_copy(peer, sp).wait_send()))
 
 
 def local(
@@ -401,7 +582,7 @@
     groups, states, channels = input_real.shape
     gp, rows, width = groups * states, residual.shape[0], residual.shape[1]
     cap = -(-max(2, 2 * rows * PICKS // n_sp) // 16) * 16
-    hidden = expert_gate.shape[2]
+    hidden, line = expert_gate.shape[2], n_sp // LO
 
     def compact(value):
         return jnp.swapaxes(value, 1, 2).reshape(chans, states)
@@ -425,8 +606,8 @@
             pltpu.VMEM((tokens, gp), f32),
             pltpu.VMEM((tokens, gp), f32),
             pltpu.VMEM((tokens, gp), f32),
-            pltpu.VMEM((4, gp), f32),
-            pltpu.VMEM((n_sp, 4, gp), f32),
+            pltpu.VMEM((3, gp), f32),
+            pltpu.VMEM((n_sp, 3, gp), f32),
             pltpu.VMEM((tokens, chans), bf16),
             pltpu.VMEM((n_tp, rows, chans), bf16),
             pltpu.VMEM((n_tp,) + projection.shape, bf16),
@@ -435,8 +616,16 @@
             pltpu.VMEM((hidden, width), bf16),
             pltpu.VMEM((rows, width), f32),
             pltpu.VMEM((rows, width), bf16),
+            pltpu.VMEM((BATCH_ROWS, n_tp * chans), bf16),
+            pltpu.VMEM((BATCH_ROWS, width), f32),
+            pltpu.VMEM((BATCH_ROWS, width), bf16),
+            pltpu.VMEM((n_sp * cap, rows), bf16),
+            pltpu.VMEM((line, LO * cap, rows), bf16),
+            pltpu.VMEM((line, rows, width) if n_sp <= 8 else (1, 16, 128), bf16),
             pltpu.VMEM((n_sp, cap, width), bf16),
             pltpu.VMEM((n_sp, cap, width), bf16),
+            pltpu.VMEM((n_sp, cap, n_tp * chans), bf16),
+            pltpu.VMEM((n_sp, cap, n_tp * chans), bf16),
             pltpu.VMEM((n_sp, cap, width), bf16),
             pltpu.VMEM((n_sp, cap, width), bf16),
             dma((len(small),)), dma((4,)),
@@ -444,6 +633,10 @@
             dma((n_tp,)), dma((n_tp,)),
             dma((PROJ_CHUNKS + 1,)), dma((PROJ_CHUNKS + 1,)),
             dma((PROJ_CHUNKS,)), dma((PROJ_CHUNKS,)),
+            dma((line,)), dma((line,)),
+            dma((line * HALVES,)), dma((line * HALVES,)),
+            dma((line * HALVES,)), dma((line * HALVES,)),
+            dma((n_sp,)), dma((n_sp,)),
             dma((n_sp,)), dma((n_sp,)),
             dma((n_sp,)), dma((n_sp,)),
         ],

time: 89.5 us -> 71 us (0.79)
  the two profiles are of different devices: /device:TPU:28 before, /device:TPU:13 now
where the time goes in v2:
time: 71 us; the launch traced here: 70.9 us
  Pallas kernels  69.2 us (97%)
  local copies, waits for them, and re-layouts  1.67 us (2%)
    pallas_call x1, Pallas kernels, local(): pl.pallas_call(functools.partial(kernel, n_sp, n_tp, groups, channels, st...  69.2 us
    unnamed x1, local copies, waits for them, and re-layouts  1.67 us

profile of v2, /device:TPU:13, one launch (start us, length us, event | category | flops | bytes accessed | tf_op | source)
XLA Modules:
  0.0 70.9 jit_solution(2059728239392603764)
XLA Ops:
  0.0 69.2 %shard_map.190 = bf16[64,2048]{1,0:T(8,128)(2,1)} custom-call(bf16[256,256]{1,0:T(8,128)(2,1)} %x_hbm.1, f32[16,256]{1,0:T(8,128)} %ret_hbm.1, f32[16,64]{1,0:T(8,128)} %real_hbm.1, f32[16,64]{1,0:T(8,128)} %freq_hbm.1, f32[1,16]{1,0:T(1,128)} %bitcast.23, f32[16,16]{1,0:T(8,128)} %skip_hbm.1, f32[1,1024]{1,0:T(1,128)} %bitcast.20, f32[256,64]{1,0:T(8,128)} %bitcast.14, ...), custom_call_target="tpu_custom_call" | custom-call | tf_op jit(solution)/shard_map/pallas_call | solution.py:599
  69.2 1.7 %copy.22 = bf16[64,2048]{1,0:T(8,128)(2,1)} copy(bf16[64,2048]{1,0:T(8,128)(2,1)} %shard_map.190) | data formatting | bytes 524288

commit v3 on v2

--- a/solution.py
+++ b/solution.py
@@ -15,9 +15,12 @@
 NT = (((1,), (1,)), ((), ()))
 TN = (((0,), (0,)), ((), ()))
 PROJ_CHUNKS = 8
-PROJ_FIRST = 3
+PROJ_RELAY = 1
+PROJ_FIRST = 1
+PROJ_NEXT = 2
+EARLY = 2
 LO = 2
-HALVES = 2
+PIECES = 4
 BATCH_ROWS = 128
 
 
@@ -72,7 +75,7 @@
     acc, hid, scaled_v, acc_b, hid_b, pick_out, pick_in, raw, res_out, res_in, y_out, y_in,
     ret_out, ret_in,
     in_sem, w_sem, car_s, car_r, mix_s, mix_r, prj_s, prj_r, fwd_s, fwd_r,
-    pick_s, pick_r, up_s, up_r, low_s, low_r, res_s, res_r, y_s, y_r, back_s, back_r,
+    rel_s, pick_s, pick_r, raw_s, raw_r, via_s, res_s, res_r, y_s, y_r, back_s, back_r,
 ):
     sp, tp = lax.axis_index("sp"), lax.axis_index("tp")
     tokens, chans = x_ref.shape
@@ -116,31 +119,51 @@
     depth = proj_ref.shape[0] // PROJ_CHUNKS
     near = tp + 1 - 2 * lax.rem(tp, 2)
     far = lax.rem(tp + 2, n_tp)
+    hi, lo = sp // LO, lax.rem(sp, LO)
+    line = n_sp // LO
+    flood = n_sp == 8
 
     def piece(i):
         return pl.ds(i * depth, depth)
 
-    proj_far = [
-        pltpu.make_async_remote_copy(
-            proj_ref.at[piece(i)], proj_all.at[tp, piece(i)], prj_s.at[i], prj_r.at[i],
+    direct = PROJ_CHUNKS - LO * PROJ_RELAY
+    relayed = [direct + PROJ_RELAY * lo + i for i in range(PROJ_RELAY)]
+    foreign = [direct + PROJ_RELAY * (1 - lo) + i for i in range(PROJ_RELAY)]
+    sent = relayed + list(range(direct))
+
+    def far_copy(c):
+        return pltpu.make_async_remote_copy(
+            proj_ref.at[piece(c)], proj_all.at[tp, piece(c)], prj_s.at[c], prj_r.at[c],
             device_id={"tp": far},
         )
-        for i in range(PROJ_CHUNKS)
-    ]
+
+    def far_chunk(c):
+        return proj_all.at[far, piece(c)]
+
+    def relay_copy(c):
+        return pltpu.make_async_remote_copy(
+            far_chunk(c), far_chunk(c), rel_s.at[c], prj_r.at[c],
+            device_id={"sp": hi * LO + 1 - lo},
+        )
+
+    def near_copy(c):
+        return pltpu.make_async_remote_copy(
+            far_chunk(c), far_chunk(c), fwd_s.at[c], fwd_r.at[c], device_id={"tp": near},
+        )
+
     proj_near = pltpu.make_async_remote_copy(
         proj_ref, proj_all.at[tp], prj_s.at[PROJ_CHUNKS], prj_r.at[PROJ_CHUNKS],
         device_id={"tp": near},
     )
-    proj_fwd = [
-        pltpu.make_async_remote_copy(
-            proj_all.at[far, piece(i)], proj_all.at[far, piece(i)], fwd_s.at[i], fwd_r.at[i],
-            device_id={"tp": near},
-        )
-        for i in range(PROJ_CHUNKS)
-    ]
-    for copy in proj_far[:PROJ_FIRST]:
-        copy.start()
-    proj_near.start()
+    for c in sent[: PROJ_RELAY + PROJ_FIRST]:
+        far_copy(c).start()
+    following = sent[PROJ_RELAY + PROJ_FIRST : PROJ_RELAY + PROJ_FIRST + PROJ_NEXT]
+
+    @pl.when(hi >= line // 2)
+    def _():
+        for c in following:
+            far_copy(c).start()
+
 
     for fetch in fetches:
         fetch.wait()
@@ -159,16 +182,22 @@
     w_high, w_low = split(weight)
 
     def every(count, width, body):
+        if flood:
+            for i in range(count // width):
+                body(pl.ds(i * width, width))
+            return
+
         def step(i, c):
             body(pl.ds(pl.multiple_of(i * width, width), width))
             return c
 
         lax.fori_loop(0, count // width, step, 0)
 
-    hi, lo = sp // LO, lax.rem(sp, LO)
-    line = n_sp // LO
-    flood = n_sp <= 8
-    piece_rows = rows // HALVES
+    piece_rows = rows // PIECES
+    mate = hi + 1 - 2 * lax.rem(hi, 2)
+    gate_node = 2 - hi // 2
+    is_gate = (hi == 1) | (hi == 2)
+    beyond = [gate_node, 3 * (1 - hi // 2)]
 
     def pick_copy(k):
         peer = lax.rem(hi + k + 1, line)
@@ -177,46 +206,42 @@
             pick_in.at[hi], pick_s.at[k], pick_r.at[k], device_id={"sp": peer * LO + lo},
         )
 
-    def hop(sign, step, part):
-        owner = lax.rem(hi - sign * step + line, line)
-        piece = pl.ds(part * piece_rows, piece_rows)
-        source = res_ref.at[piece] if step == 0 else raw.at[owner, piece]
-        s_sem, r_sem = (up_s, up_r) if sign > 0 else (low_s, low_r)
-        at = step * HALVES + part
-        return pltpu.make_async_remote_copy(
-            source, raw.at[owner, piece], s_sem.at[at], r_sem.at[at],
-            device_id={"sp": lax.rem(sp + sign * LO + n_sp, n_sp)},
-        )
-
-    def inside(value):
-        return (value >= 0) & (value < line)
-
-    def hop_start(step, part):
-        for sign in (1, -1):
-            @pl.when(inside(hi - sign * step) & inside(hi + sign))
-            def _():
-                hop(sign, step, part).start()
-
-    def hop_sent(step, part):
-        for sign in (1, -1):
-            @pl.when(inside(hi - sign * step) & inside(hi + sign))
-            def _():
-                hop(sign, step, part).wait_send()
-
-    def hop_pass(step, part):
-        for sign in (1, -1):
-            @pl.when(inside(hi - sign * (step + 1)))
-            def _():
-                owner = lax.rem(hi - sign * (step + 1) + line, line)
-                piece = pl.ds(part * piece_rows, piece_rows)
-                s_sem, r_sem = (up_s, up_r) if sign > 0 else (low_s, low_r)
-                at = step * HALVES + part
-                pltpu.make_async_remote_copy(
-                    raw.at[owner, piece], raw.at[owner, piece], s_sem.at[at], r_sem.at[at],
-                    device_id={"sp": lax.rem(sp + LO, n_sp)},
-                ).wait_recv()
-        if step + 1 < line - 1:
-            hop_start(step + 1, part)
+    def rows_at(part):
+        return pl.ds(part * piece_rows, piece_rows)
+
+    def raw_copy(kind, part):
+        return pltpu.make_async_remote_copy(
+            res_ref.at[rows_at(part)], raw.at[hi, rows_at(part)],
+            raw_s.at[kind * PIECES + part], raw_r.at[hi * PIECES + part],
+            device_id={"sp": (gate_node if kind == 0 else mate) * LO + lo},
+        )
+
+    def via_copy(i, part):
+        owner = beyond[i]
+        return pltpu.make_async_remote_copy(
+            raw.at[owner, rows_at(part)], raw.at[owner, rows_at(part)],
+            via_s.at[i * PIECES + part], raw_r.at[owner * PIECES + part],
+            device_id={"sp": mate * LO + lo},
+        )
+
+    def raw_start(kind, part, upward):
+        node = mate if kind else gate_node
+
+        @pl.when(node > hi if upward else node < hi)
+        def _():
+            raw_copy(kind, part).start()
+
+    def raw_arrived(owner, part):
+        pltpu.make_async_remote_copy(
+            raw.at[owner, rows_at(part)], raw.at[owner, rows_at(part)],
+            raw_s.at[part], raw_r.at[owner * PIECES + part], device_id={"sp": mate * LO + lo},
+        ).wait_recv()
+
+    def forward(i, part):
+        @pl.when(is_gate)
+        def _():
+            raw_arrived(beyond[i], part)
+            via_copy(i, part).start()
 
     def res_copy(owner):
         return pltpu.make_async_remote_copy(
@@ -233,12 +258,8 @@
         res_in[owner * LO + lo] = res_out[owner * LO + lo]
         res_copy(owner).start()
 
-    def share_line(step):
-        for sign in (1, -1):
-            @pl.when(inside(hi - sign * step))
-            def _():
-                owner = lax.rem(hi - sign * step + line, line)
-                share(owner, pick_in[owner], raw.at[owner])
+    def share_line(owner):
+        share(owner, pick_in[owner], raw.at[owner])
 
     def send_res(k):
         peer = lax.rem(sp + k + 1, n_sp)
@@ -249,7 +270,18 @@
     pick_out[...] = chosen
     if flood:
         repeat(line - 1, lambda k: pick_copy(k).start())
-        hop_start(0, 0)
+        for kind in (1, 0):
+            for part in range(PIECES):
+                raw_start(kind, part, False)
+
+        @pl.when(hi > 0)
+        def _():
+            for part in range(3):
+                raw_start(0, part, True)
+
+        for part in range(EARLY):
+            raw_start(1, part, True)
+        share(hi, pick_out[pl.ds(pl.multiple_of(hi * LO * cap, LO * cap), LO * cap), :], res_ref)
     else:
         def spread_res(cols):
             res_out[:, :, cols] = dot(chosen, res_ref[:, cols]).astype(bf16).reshape(n_sp, cap, 256)
@@ -310,8 +342,11 @@
     for bar, d_ref in ((bar_re, d_re), (bar_im, d_im)):
         high, low = wide(bar)
         d_ref[...] = dot(x, high) + dot(x, low)
-    held = dot(jnp.exp(ret_ref[...]), perm.astype(f32), NT, precision=highest)
-    shr[...] = dot(held, widen, TN, precision=highest)
+    held = jnp.exp(ret_ref[...])
+    first_part = held.astype(bf16)
+    rest = held - first_part.astype(f32)
+    held = dot(jnp.concatenate([first_part, *split(rest)], axis=0), perm, NT).astype(bf16)
+    shr[...] = dot(held, jnp.concatenate([widen.astype(bf16)] * 3, axis=0), TN)
 
     k_re = jnp.broadcast_to(k_re, (SPANS, gp))
     k_im = jnp.broadcast_to(k_im, (SPANS, gp))
@@ -368,10 +403,22 @@
         def _():
             carry_copy(k).wait_send()
 
-    repeat(n_sp - 1, carry_start)
+    repeat(n_sp - 1, lambda k: carry_start(n_sp - 2 - k))
     if flood:
-        for part in range(1, HALVES):
-            hop_start(0, part)
+        for part in range(EARLY, PIECES):
+            raw_start(1, part, True)
+
+        @pl.when(hi > 0)
+        def _():
+            for part in range(3, PIECES):
+                raw_start(0, part, True)
+
+        @pl.when(hi == 0)
+        def _():
+            for part in range(PIECES):
+                raw_copy(0, part).start()
+
+        forward(0, 0)
     c_re, c_im, s_re, s_im = [
         jnp.concatenate([entry[i] for entry in entries], axis=0) for i in range(4)
     ]
@@ -385,12 +432,14 @@
     skip = jnp.sum(skip, axis=0, keepdims=True)
 
     if flood:
-        share(hi, pick_out[pl.ds(pl.multiple_of(hi * LO * cap, LO * cap), LO * cap), :], res_ref)
-        hop_pass(0, 0)
+        forward(0, 1)
     repeat(n_sp - 1, carry_arrived)
     if flood:
-        for part in range(1, HALVES):
-            hop_pass(0, part)
+        forward(0, 2)
+    for c in relayed:
+        far_copy(c).wait_recv()
+        relay_copy(c).start()
+        near_copy(c).start()
 
     def fold(position, state):
         part = carry_in[position]
@@ -437,13 +486,24 @@
             )
         )
         mixes[-1].start()
-    for copy in proj_far[PROJ_FIRST:]:
-        copy.start()
+
+    @pl.when(hi < line // 2)
+    def _():
+        for c in following:
+            far_copy(c).start()
+
+    for c in sent[PROJ_RELAY + PROJ_FIRST + PROJ_NEXT :]:
+        far_copy(c).start()
+    proj_near.start()
     mix_in[tp] = mix_out[mine(tp), :]
     if flood:
+        forward(0, 3)
+        forward(1, 0)
         repeat(line - 1, lambda k: pick_copy(k).wait_recv())
-        hop_pass(1, 0)
-        share_line(1)
+        for part in range(PIECES):
+            raw_arrived(mate, part)
+        share_line(mate)
+        forward(1, 1)
     for copy in mixes:
         copy.wait_recv()
 
@@ -458,13 +518,13 @@
     home = sp // take
 
     def batch_of(i):
-        return lax.rem(home + batches // 2 + i, batches) if batches > 1 else 0
-
-    def others(i, body):
+        return lax.rem(home + i, batches) if batches > 1 else 0
+
+    def others(i, body, backward=False):
         base = batch_of(i) * take
 
         def one(j):
-            peer = base + j
+            peer = base + (take - 1 - j if backward else j)
 
             @pl.when(peer != sp)
             def _():
@@ -477,24 +537,54 @@
             y_out.at[peer], y_in.at[source], y_s.at[peer], y_r.at[source], device_id={"sp": peer}
         )
 
-    repeat(batches, lambda i: others(i, lambda peer: y_copy(peer, sp).start()))
+    def y_start(i):
+        outward = home < batches // 2
+
+        @pl.when(outward)
+        def _():
+            others(i, lambda peer: y_copy(peer, sp).start(), True)
+
+        @pl.when(~outward)
+        def _():
+            others(i, lambda peer: y_copy(peer, sp).start())
+
+    repeat(batches, lambda i: y_start(batches - 1 - i))
     y_in[sp] = y_out[sp]
 
+    def project_arrived(chunks):
+        for c in chunks:
+            far_copy(c).wait_recv()
+            near_copy(c).start()
+
+    def far_share(i):
+        @pl.when(~is_gate)
+        def _():
+            for part in range(PIECES):
+                raw_arrived(beyond[i], part)
+
+        share_line(beyond[i])
+
     if flood:
-        for part in range(1, HALVES):
-            hop_pass(1, part)
-        share_line(2)
-        for step in range(2, line - 1):
-            for part in range(HALVES):
-                hop_pass(step, part)
-            share_line(step + 1)
-    for i in range(PROJ_CHUNKS):
-        proj_far[i].wait_recv()
-        proj_fwd[i].start()
+        far_share(0)
+        forward(1, 2)
+        forward(1, 3)
+
+        @pl.when(is_gate)
+        def _():
+            far_share(1)
+
+        project_arrived(list(range(direct)) + foreign)
+
+        @pl.when(~is_gate)
+        def _():
+            far_share(1)
+
+    else:
+        project_arrived(list(range(direct)) + foreign)
     own.wait()
     proj_near.wait_recv()
-    for copy in proj_fwd:
-        copy.wait_recv()
+    for c in range(PROJ_CHUNKS):
+        near_copy(c).wait_recv()
     if flood:
         for owner in range(line):
             res_copy(owner).wait_recv()
@@ -556,14 +646,27 @@
     every(width, 256, combine)
     o_ref[...] = layer_norm(acc[...], final_gain_ref[...]).astype(bf16)
 
-    for copy in proj_far + [proj_near] + proj_fwd + mixes:
+    for c in sent:
+        far_copy(c).wait_send()
+    for c in relayed:
+        relay_copy(c).wait_send()
+    for c in range(PROJ_CHUNKS):
+        near_copy(c).wait_send()
+    for copy in [proj_near] + mixes:
         copy.wait_send()
     repeat(n_sp - 1, carry_sent)
     if flood:
         repeat(line - 1, lambda k: pick_copy(k).wait_send())
-        for step in range(line - 1):
-            for part in range(HALVES):
-                hop_sent(step, part)
+        for part in range(PIECES):
+            for kind in range(2):
+                raw_copy(kind, part).wait_send()
+
+        @pl.when(is_gate)
+        def _():
+            for part in range(PIECES):
+                for i in range(2):
+                    via_copy(i, part).wait_send()
+
         for owner in range(line):
             res_copy(owner).wait_send()
     else:
@@ -621,7 +724,7 @@
             pltpu.VMEM((BATCH_ROWS, width), bf16),
             pltpu.VMEM((n_sp * cap, rows), bf16),
             pltpu.VMEM((line, LO * cap, rows), bf16),
-            pltpu.VMEM((line, rows, width) if n_sp <= 8 else (1, 16, 128), bf16),
+            pltpu.VMEM((line, rows, width) if n_sp == 8 else (1, 16, 128), bf16),
             pltpu.VMEM((n_sp, cap, width), bf16),
             pltpu.VMEM((n_sp, cap, width), bf16),
             pltpu.VMEM((n_sp, cap, n_tp * chans), bf16),
@@ -633,9 +736,8 @@
             dma((n_tp,)), dma((n_tp,)),
             dma((PROJ_CHUNKS + 1,)), dma((PROJ_CHUNKS + 1,)),
             dma((PROJ_CHUNKS,)), dma((PROJ_CHUNKS,)),
-            dma((line,)), dma((line,)),
-            dma((line * HALVES,)), dma((line * HALVES,)),
-            dma((line * HALVES,)), dma((line * HALVES,)),
+            dma((PROJ_CHUNKS,)), dma((line,)), dma((line,)),
+            dma((2 * PIECES,)), dma((line * PIECES,)), dma((2 * PIECES,)),
             dma((n_sp,)), dma((n_sp,)),
             dma((n_sp,)), dma((n_sp,)),
             dma((n_sp,)), dma((n_sp,)),

time: 71 us -> 65.3 us (0.920)
  the two profiles are of different devices: /device:TPU:13 before, /device:TPU:28 now
where the time goes in v3:
time: 65.3 us; the launch traced here: 64.7 us
  Pallas kernels  63 us (96%)
  local copies, waits for them, and re-layouts  1.67 us (3%)
    pallas_call x1, Pallas kernels, local(): pl.pallas_call(functools.partial(kernel, n_sp, n_tp, groups, channels, st...  63 us
    unnamed x1, local copies, waits for them, and re-layouts  1.67 us

profile of v3, /device:TPU:28, one launch (start us, length us, event | category | flops | bytes accessed | tf_op | source)
XLA Modules:
  0.0 64.7 jit_solution(6097180945531693407)
XLA Ops:
  0.0 63.0 %shard_map.190 = bf16[64,2048]{1,0:T(8,128)(2,1)} custom-call(bf16[256,256]{1,0:T(8,128)(2,1)} %x_hbm.1, f32[16,256]{1,0:T(8,128)} %ret_hbm.1, f32[16,64]{1,0:T(8,128)} %real_hbm.1, f32[16,64]{1,0:T(8,128)} %freq_hbm.1, f32[1,16]{1,0:T(1,128)} %bitcast.23, f32[16,16]{1,0:T(8,128)} %skip_hbm.1, f32[1,1024]{1,0:T(1,128)} %bitcast.20, f32[256,64]{1,0:T(8,128)} %bitcast.14, ...), custom_call_target="tpu_custom_call" | custom-call | tf_op jit(solution)/shard_map/pallas_call | solution.py:702
  63.0 1.7 %copy.22 = bf16[64,2048]{1,0:T(8,128)(2,1)} copy(bf16[64,2048]{1,0:T(8,128)(2,1)} %shard_map.190) | data formatting | bytes 524288

commit v4 on v3

--- a/solution.py
+++ b/solution.py
@@ -19,6 +19,7 @@
 PROJ_FIRST = 1
 PROJ_NEXT = 2
 EARLY = 2
+DIRECT_SHARE = 2
 LO = 2
 PIECES = 4
 BATCH_ROWS = 128
@@ -73,9 +74,9 @@
     out_re_ref, out_im_ref, res_ref, mix_gain_ref, routes_ref, rw_ref, final_gain_ref,
     d_re, d_im, shr, carry_out, carry_in, mix_out, mix_in, proj_all, gate_v, up_v, down_v,
     acc, hid, scaled_v, acc_b, hid_b, pick_out, pick_in, raw, res_out, res_in, y_out, y_in,
-    ret_out, ret_in,
+    ret_out, ret_in, w_out, gate_w, gate_in, gate_out, sum_in,
     in_sem, w_sem, car_s, car_r, mix_s, mix_r, prj_s, prj_r, fwd_s, fwd_r,
-    rel_s, pick_s, pick_r, raw_s, raw_r, via_s, res_s, res_r, y_s, y_r, back_s, back_r,
+    rel_s, pick_s, pick_r, raw_s, raw_r, via_s, res_s, res_r, y_s, y_r, back_s, back_r, gw_s, gw_r, gc_s, gc_r, sum_s, sum_r,
 ):
     sp, tp = lax.axis_index("sp"), lax.axis_index("tp")
     tokens, chans = x_ref.shape
@@ -267,7 +268,47 @@
             res_out.at[peer], res_in.at[sp], res_s.at[k], res_r.at[k], device_id={"sp": peer}
         )
 
+    take = BATCH_ROWS // cap
+    batches = n_sp // take
+    home = sp // take
+
+    def batch_of(i):
+        return lax.rem(home + i, batches) if batches > 1 else 0
+
+    close, apart = home * take, batch_of(1) * take
+    keep = width // DIRECT_SHARE if flood else width
+    turn = hi // 2
+    order = (1 - turn, turn)
+
+    def their_weight():
+        slab = pl.ds(pl.multiple_of(apart * cap, BATCH_ROWS), BATCH_ROWS)
+        return pltpu.make_async_remote_copy(
+            w_out.at[:, slab], gate_w.at[lax.rem(hi, 2)], gw_s.at[0], gw_r.at[lax.rem(hi, 2)],
+            device_id={"sp": gate_node * LO + lo},
+        )
+
+    def part_copy(t, column, way):
+        return pltpu.make_async_remote_copy(
+            ret_out.at[apart + LO * t + column, :, pl.ds(keep, width - keep)],
+            gate_in.at[t, sp - close], gc_s.at[2 * way + t], gc_r.at[t * take + sp - close],
+            device_id={"sp": (1 + turn) * LO + column},
+        )
+
+    def part_arrived(t, c):
+        pltpu.make_async_remote_copy(
+            gate_in.at[t, c], gate_in.at[t, c], gc_s.at[0], gc_r.at[t * take + c],
+            device_id={"sp": mate * LO + lo},
+        ).wait_recv()
+
+    def sum_copy(t):
+        return pltpu.make_async_remote_copy(
+            gate_out.at[t], sum_in, sum_s.at[t], sum_r.at[0],
+            device_id={"sp": apart + LO * t + lo},
+        )
+
     pick_out[...] = chosen
+    w_out[0] = w_high
+    w_out[1] = w_low
     if flood:
         repeat(line - 1, lambda k: pick_copy(k).start())
         for kind in (1, 0):
@@ -513,13 +554,6 @@
             dot(chosen, mix_in[part]).astype(bf16).reshape(n_sp, cap, chans)
         )
 
-    take = BATCH_ROWS // cap
-    batches = n_sp // take
-    home = sp // take
-
-    def batch_of(i):
-        return lax.rem(home + i, batches) if batches > 1 else 0
-
     def others(i, body, backward=False):
         base = batch_of(i) * take
 
@@ -585,14 +619,6 @@
     proj_near.wait_recv()
     for c in range(PROJ_CHUNKS):
         near_copy(c).wait_recv()
-    if flood:
-        for owner in range(line):
-            res_copy(owner).wait_recv()
-    else:
-        repeat(n_sp - 1, lambda k: send_res(k).wait_recv())
-    for copy in loads[1:]:
-        copy.wait()
-
     def hidden_of(y, scaled_ref, acc_ref, residual_of):
         squares = jnp.sum(y * y, axis=1, keepdims=True)
         scaled_ref[...] = (y * gain_ref[...]).astype(bf16)
@@ -606,36 +632,104 @@
         every(width, 256, project)
         return layer_norm(acc_ref[...], mix_gain_ref[...]).astype(bf16)
 
-    def back_copy(peer, source):
-        return pltpu.make_async_remote_copy(
-            ret_out.at[peer], ret_in.at[source], back_s.at[peer], back_r.at[source],
-            device_id={"sp": peer},
-        )
-
-    def expert(i):
-        base = batch_of(i) * take
-        these = pl.ds(base, take)
-        others(i, lambda peer: y_copy(peer, peer).wait_recv())
-        y = y_in[these].reshape(BATCH_ROWS, total_chans).astype(f32)
-        hid_b[...] = hidden_of(
-            y, scaled_v, acc_b, lambda cols: res_in[these, :, cols].reshape(BATCH_ROWS, 256)
-        )
-        gate, up = dot(hid_b[...], gate_v[...]), dot(hid_b[...], up_v[...])
+    def back_copy(peer, source, columns=None):
+        cols = pl.ds(0, columns or width)
+        return pltpu.make_async_remote_copy(
+            ret_out.at[peer, :, cols], ret_in.at[source, :, cols],
+            back_s.at[peer], back_r.at[source], device_id={"sp": peer},
+        )
+
+    def far_back(body):
+        for t in order:
+            for column in range(LO):
+                body(apart + LO * t + column)
+
+    def expert(sources, way=None):
+        count = len(sources) * cap
+        for source in sources:
+            @pl.when(source != sp)
+            def _():
+                y_copy(source, source).wait_recv()
+        top = pl.ds(0, count)
+        y = jnp.concatenate([y_in[source] for source in sources], axis=0).astype(f32)
+        hid_b[top, :] = hidden_of(
+            y, scaled_v.at[top], acc_b.at[top],
+            lambda cols: jnp.concatenate([res_in[source, :, cols] for source in sources], axis=0),
+        )
+        rows_b = hid_b[top, :]
+        gate, up = dot(rows_b, gate_v[...]), dot(rows_b, up_v[...])
         active = (gate * jax.nn.sigmoid(gate) * up).astype(bf16)
 
         def produce(cols):
-            ret_out[these, :, cols] = (
-                dot(active, down_v[:, cols]).astype(bf16).reshape(take, cap, 256)
-            )
+            made = dot(active, down_v[:, cols]).astype(bf16)
+            for j, source in enumerate(sources):
+                ret_out[source, :, cols] = made[j * cap : (j + 1) * cap]
 
         every(width, 256, produce)
-        others(i, lambda peer: back_copy(peer, sp).start())
-
-    repeat(batches, expert)
+        if way is None:
+            for source in sources:
+                @pl.when(source != sp)
+                def _():
+                    back_copy(source, sp).start()
+            return
+        column = lo if way == 0 else 1 - lo
+        for t, source in zip(order, sources):
+            if way == 0:
+                @pl.when(is_gate)
+                def _():
+                    gate_in[t, sp - close] = ret_out[source, :, pl.ds(keep, width - keep)]
+
+                @pl.when(~is_gate)
+                def _():
+                    part_copy(t, column, way).start()
+            else:
+                part_copy(t, column, way).start()
+        for source in sources:
+            back_copy(source, sp, keep).start()
+
+    def sum_ready(t):
+        for c in range(take):
+            @pl.when(c != sp - close)
+            def _():
+                part_arrived(t, c)
+        pltpu.make_async_remote_copy(
+            gate_w.at[t], gate_w.at[t], gw_s.at[0], gw_r.at[t], device_id={"sp": mate * LO + lo},
+        ).wait_recv()
+        got = gate_in[t].reshape(BATCH_ROWS, width - keep)
+        whole = dot(gate_w[t, 0], got, TN) + dot(gate_w[t, 1], got, TN)
+        gate_out[t] = whole.astype(bf16)
+        sum_copy(t).start()
+
+    if flood:
+        for copy in loads[1:]:
+            copy.wait()
+        their_weight().start()
+        expert([apart + LO * t + lo for t in order], 0)
+        for owner in beyond:
+            res_copy(owner).wait_recv()
+        expert([apart + LO * t + 1 - lo for t in order], 1)
+        for owner in (hi, mate):
+            res_copy(owner).wait_recv()
+        expert([close + j for j in range(take)])
+    else:
+        repeat(n_sp - 1, lambda k: send_res(k).wait_recv())
+        for copy in loads[1:]:
+            copy.wait()
+        repeat(batches, lambda i: expert([batch_of(i) * take + j for j in range(take)]))
     ret_in[sp] = ret_out[sp]
     y = jnp.concatenate([mix_in[part].astype(f32) for part in range(n_tp)], axis=1)
     hid[...] = hidden_of(y, scaled_v.at[pl.ds(0, rows)], acc, lambda cols: res_ref[:, cols])
-    repeat(batches, lambda i: others(i, lambda peer: back_copy(peer, peer).wait_recv()))
+    if flood:
+        @pl.when(is_gate)
+        def _():
+            for t in order:
+                sum_ready(t)
+
+        others(0, lambda peer: back_copy(peer, peer).wait_recv())
+        far_back(lambda peer: back_copy(peer, peer, keep).wait_recv())
+        sum_copy(0).wait_recv()
+    else:
+        repeat(batches, lambda i: others(i, lambda peer: back_copy(peer, peer).wait_recv()))
 
     def combine(cols):
         got = ret_in[:, :, cols].reshape(slots, 256)
@@ -643,7 +737,19 @@
             deep_alpha * hid[:, cols].astype(f32) + dot(w_high, got, TN) + dot(w_low, got, TN)
         )
 
-    every(width, 256, combine)
+    def combine_close(cols):
+        got = ret_in[pl.ds(close, take), :, pl.ds(cols.start + keep, cols.size)]
+        got = got.reshape(BATCH_ROWS, cols.size)
+        slab = pl.ds(pl.multiple_of(close * cap, BATCH_ROWS), BATCH_ROWS)
+        there = pl.ds(cols.start + keep, cols.size)
+        acc[:, there] = (
+            deep_alpha * hid[:, there].astype(f32) + sum_in[:, cols].astype(f32)
+            + dot(w_out[0, slab, :], got, TN) + dot(w_out[1, slab, :], got, TN)
+        )
+
+    every(keep, 256, combine)
+    if flood:
+        every(width - keep, 256, combine_close)
     o_ref[...] = layer_norm(acc[...], final_gain_ref[...]).astype(bf16)
 
     for c in sent:
@@ -672,7 +778,22 @@
     else:
         repeat(n_sp - 1, lambda k: send_res(k).wait_send())
     repeat(batches, lambda i: others(i, lambda peer: y_copy(peer, sp).wait_send()))
-    repeat(batches, lambda i: others(i, lambda peer: back_copy(peer, sp).wait_send()))
+    if flood:
+        others(0, lambda peer: back_copy(peer, sp).wait_send())
+        far_back(lambda peer: back_copy(peer, sp, keep).wait_send())
+        their_weight().wait_send()
+        for t in range(2):
+            @pl.when(~is_gate)
+            def _():
+                part_copy(t, lo, 0).wait_send()
+
+            part_copy(t, 1 - lo, 1).wait_send()
+
+            @pl.when(is_gate)
+            def _():
+                sum_copy(t).wait_send()
+    else:
+        repeat(batches, lambda i: others(i, lambda peer: back_copy(peer, sp).wait_send()))
 
 
 def local(
@@ -686,6 +807,8 @@
     gp, rows, width = groups * states, residual.shape[0], residual.shape[1]
     cap = -(-max(2, 2 * rows * PICKS // n_sp) // 16) * 16
     hidden, line = expert_gate.shape[2], n_sp // LO
+    take = BATCH_ROWS // cap
+    rest = width - width // DIRECT_SHARE if n_sp == 8 else 128
 
     def compact(value):
         return jnp.swapaxes(value, 1, 2).reshape(chans, states)
@@ -731,6 +854,11 @@
             pltpu.VMEM((n_sp, cap, n_tp * chans), bf16),
             pltpu.VMEM((n_sp, cap, width), bf16),
             pltpu.VMEM((n_sp, cap, width), bf16),
+            pltpu.VMEM((2, n_sp * cap, rows), bf16),
+            pltpu.VMEM((2, 2, take * cap, rows), bf16),
+            pltpu.VMEM((2, take, cap, rest), bf16),
+            pltpu.VMEM((2, rows, rest), bf16),
+            pltpu.VMEM((rows, rest), bf16),
             dma((len(small),)), dma((4,)),
             dma((n_sp,)), dma((n_sp,)),
             dma((n_tp,)), dma((n_tp,)),
@@ -741,6 +869,7 @@
             dma((n_sp,)), dma((n_sp,)),
             dma((n_sp,)), dma((n_sp,)),
             dma((n_sp,)), dma((n_sp,)),
+            dma((1,)), dma((2,)), dma((4,)), dma((2 * take,)), dma((2,)), dma((1,)),
         ],
         compiler_params=pltpu.CompilerParams(
             collective_id=0, has_side_effects=True, vmem_limit_bytes=60 * 1024 * 1024

time: 65.3 us -> 61.2 us (0.937)
  the two profiles are of different devices: /device:TPU:28 before, /device:TPU:16 now
where the time goes in v4:
time: 61.2 us; the launch traced here: 61.1 us
  Pallas kernels  59.4 us (97%)
  local copies, waits for them, and re-layouts  1.67 us (3%)
    pallas_call x1, Pallas kernels, local(): pl.pallas_call(functools.partial(kernel, n_sp, n_tp, groups, channels, st...  59.4 us
    unnamed x1, local copies, waits for them, and re-layouts  1.67 us

profile of v4, /device:TPU:16, one launch (start us, length us, event | category | flops | bytes accessed | tf_op | source)
XLA Modules:
  0.0 61.1 jit_solution(16167217046818206932)
XLA Ops:
  0.0 59.4 %shard_map.190 = bf16[64,2048]{1,0:T(8,128)(2,1)} custom-call(bf16[256,256]{1,0:T(8,128)(2,1)} %x_hbm.1, f32[16,256]{1,0:T(8,128)} %ret_hbm.1, f32[16,64]{1,0:T(8,128)} %real_hbm.1, f32[16,64]{1,0:T(8,128)} %freq_hbm.1, f32[1,16]{1,0:T(1,128)} %bitcast.23, f32[16,16]{1,0:T(8,128)} %skip_hbm.1, f32[1,1024]{1,0:T(1,128)} %bitcast.20, f32[256,64]{1,0:T(8,128)} %bitcast.14, ...), custom_call_target="tpu_custom_call" | custom-call | tf_op jit(solution)/shard_map/pallas_call | solution.py:825
  59.4 1.7 %copy.22 = bf16[64,2048]{1,0:T(8,128)(2,1)} copy(bf16[64,2048]{1,0:T(8,128)(2,1)} %shard_map.190) | data formatting | bytes 524288

commit v5 on v4

--- a/solution.py
+++ b/solution.py
@@ -454,11 +454,6 @@
             for part in range(3, PIECES):
                 raw_start(0, part, True)
 
-        @pl.when(hi == 0)
-        def _():
-            for part in range(PIECES):
-                raw_copy(0, part).start()
-
         forward(0, 0)
     c_re, c_im, s_re, s_im = [
         jnp.concatenate([entry[i] for entry in entries], axis=0) for i in range(4)
@@ -537,6 +532,12 @@
         far_copy(c).start()
     proj_near.start()
     mix_in[tp] = mix_out[mine(tp), :]
+    if flood:
+        @pl.when(hi == 0)
+        def _():
+            for part in range(PIECES):
+                raw_copy(0, part).start()
+
     if flood:
         forward(0, 3)
         forward(1, 0)
@@ -547,6 +548,11 @@
         forward(1, 1)
     for copy in mixes:
         copy.wait_recv()
+    if flood:
+        @pl.when(hi == 0)
+        def _():
+            for part in range(PIECES):
+                raw_arrived(beyond[0], part)
 
     total_chans = n_tp * chans
     for part in range(n_tp):
@@ -582,6 +588,9 @@
         def _():
             others(i, lambda peer: y_copy(peer, sp).start())
 
+    if flood:
+        forward(1, 2)
+        forward(1, 3)
     repeat(batches, lambda i: y_start(batches - 1 - i))
     y_in[sp] = y_out[sp]
 
@@ -591,7 +600,7 @@
             near_copy(c).start()
 
     def far_share(i):
-        @pl.when(~is_gate)
+        @pl.when(~is_gate & ((hi > 0) | (i > 0)))
         def _():
             for part in range(PIECES):
                 raw_arrived(beyond[i], part)
@@ -600,8 +609,6 @@
 
     if flood:
         far_share(0)
-        forward(1, 2)
-        forward(1, 3)
 
         @pl.when(is_gate)
         def _():
@@ -684,8 +691,19 @@
                     part_copy(t, column, way).start()
             else:
                 part_copy(t, column, way).start()
-        for source in sources:
-            back_copy(source, sp, keep).start()
+        if way == 0:
+            @pl.when(is_gate)
+            def _():
+                for source in sources:
+                    back_copy(source, sp, keep).start()
+        else:
+            @pl.when(~is_gate)
+            def _():
+                for t in order:
+                    back_copy(apart + LO * t + lo, sp, keep).start()
+
+            for source in sources:
+                back_copy(source, sp, keep).start()
 
     def sum_ready(t):
         for c in range(take):

time: 61.2 us -> 59.6 us (0.974)
  the two profiles are of different devices: /device:TPU:16 before, /device:TPU:0 now
where the time goes in v5:
time: 59.6 us; the launch traced here: 59.4 us
  Pallas kernels  57.7 us (97%)
  local copies, waits for them, and re-layouts  1.67 us (3%)
    pallas_call x1, Pallas kernels, local(): pl.pallas_call(functools.partial(kernel, n_sp, n_tp, groups, channels, st...  57.7 us
    unnamed x1, local copies, waits for them, and re-layouts  1.67 us

profile of v5, /device:TPU:0, one launch (start us, length us, event | category | flops | bytes accessed | tf_op | source)
XLA Modules:
  0.0 59.4 jit_solution(10598090487384554460)
XLA Ops:
  0.0 57.7 %shard_map.190 = bf16[64,2048]{1,0:T(8,128)(2,1)} custom-call(bf16[256,256]{1,0:T(8,128)(2,1)} %x_hbm.1, f32[16,256]{1,0:T(8,128)} %ret_hbm.1, f32[16,64]{1,0:T(8,128)} %real_hbm.1, f32[16,64]{1,0:T(8,128)} %freq_hbm.1, f32[1,16]{1,0:T(1,128)} %bitcast.23, f32[16,16]{1,0:T(8,128)} %skip_hbm.1, f32[1,1024]{1,0:T(1,128)} %bitcast.20, f32[256,64]{1,0:T(8,128)} %bitcast.14, ...), custom_call_target="tpu_custom_call" | custom-call | tf_op jit(solution)/shard_map/pallas_call | solution.py:843
  57.8 1.7 %copy.22 = bf16[64,2048]{1,0:T(8,128)(2,1)} copy(bf16[64,2048]{1,0:T(8,128)(2,1)} %shard_map.190) | data formatting | bytes 524288
